TPU v7x, 128 devices: a whole 4x4x4 slice. The times are simulated.
128 devices in a mesh: ep: 32 (over z, y, core), tp: 4 (over x).
Axes of the slice: x: 4, y: 4, z: 4, core: 2. Of those that a mesh axis runs over, the one named last changes fastest.
Arguments:
- conv_value: bfloat16 [49152, 2048], P(('ep', 'tp')), may hold values from -6 to 6
- conv_gate: bfloat16 [49152, 2048], P(('ep', 'tp')), may hold values from -6 to 6
- conv_taps: float32 [31, 2048], replicated, may hold values from -1 to 1
- conv_gain: float32 [2048], replicated, may hold values from 0.1 to 1.9
- conv_bias: float32 [2048], replicated, may hold values from -3 to 3
- conv_projection: bfloat16 [2048, 4096], P(None, 'tp'), may hold values from -0.125 to 0.125
- expert_input: bfloat16 [16384, 4096], P('ep'), may hold values from -6 to 6
- expert_gain: float32 [4096], replicated, may hold values from 0.1 to 1.9
- route_experts: int32 [16384, 2], P('ep'), may hold values from 0 to 31, all different within a row; in each aligned block of 128 rows (0 to 127, 128 to 255, ...) at most 16 rows name the same one
- group_gate: float32 [16384], P('ep'), may hold values from 0.3 to 1
- expert_gate: float32 [16384, 2], P('ep'), may hold values from 0.1 to 1
- gate_weight: bfloat16 [32, 4096, 1024], P('ep', None, 'tp'), may hold values from -0.09375 to 0.09375
- up_weight: bfloat16 [32, 4096, 1024], P('ep', None, 'tp'), may hold values from -0.09375 to 0.09375
- down_weight: bfloat16 [32, 1024, 4096], P('ep', None, 'tp'), may hold values from -0.1875 to 0.1875
Outputs:
- conv_out: bfloat16 [49152, 4096], P('ep', 'tp')
- expert_out: bfloat16 [16384, 4096], P('ep', 'tp')
Inputs may be any that keep to these rules, and one draw needn't show every extreme that they name: `route_experts`: each row names 2 different experts; in each aligned block of 128 rows no expert is named more than 16 times, and in some blocks one expert is named exactly 16 times.
All inputs are finite; a program needn't handle non-finite values.
Results may differ from a plain program's by a relative error of at most 0.0071.
Values may be sent and summed in bfloat16 or wider, within the bound.
A program may use at most 128 MiB of HBM per device.

v0:
```python
import jax
import jax.numpy as jnp
from jax import lax
from jax.sharding import Mesh
from jax.sharding import PartitionSpec as P

EXPERTS = 32
TOP = 2
MOE_DEV = 128
CAP = 16
EP_TP = ("ep_0", "ep_1", "ep_2", "tp")
EP = ("ep_0", "ep_1", "ep_2")


epsilon = 1e-06


def passed_along(value, axis, steps):
    count = lax.axis_size(axis)
    leading, last = (max(0, -steps), min(count, count - steps))
    return lax.ppermute(value, axis, [(source, source + steps) for source in range(leading, last)])


def joined_along(blocks, dim):
    shape = list(blocks.shape[1:])
    shape[dim] *= blocks.shape[0]
    return jnp.moveaxis(blocks, 0, dim).reshape(shape)


def work_in_pieces(x, axis, dim, apply, out_dim):
    size, rows = (lax.axis_size(axis), x.shape[dim])
    count = 2 if rows % 2 == 0 else 1
    outs, length = ([], rows // count)
    for k in range(count):
        section = lax.slice_in_dim(x, k * length, (k + 1) * length, axis=dim)
        starts = jnp.arange(size) * rows + k * length
        outs.append(jax.vmap(apply)(lax.all_gather(section, axis), starts))
    return joined_along(jnp.concatenate(outs, axis=out_dim + 1), out_dim)


def split_up(x, dim, length):
    before, after = (x.shape[:dim], x.shape[dim + 1 :])
    return jnp.moveaxis(x.reshape(*before, length, -1, *after), dim, 0)


def exchange_in_order(blocks, axes, order):
    shape = [lax.axis_size(a) for a in axes]
    blocks = blocks.reshape(*shape, *blocks.shape[1:])
    for k in order:
        blocks = lax.all_to_all(blocks, axes[k], split_axis=k, concat_axis=k, tiled=True)
    return blocks.reshape(-1, *blocks.shape[len(axes) :])


def core_and_chips(x, groups, order, split_dim, concat_dim):
    length = lax.axis_size(groups[0]) * lax.axis_size(groups[1])
    blocks = split_up(x, split_dim, length)
    return joined_along(exchange_in_order(blocks, groups, order), concat_dim)


def root_mean_norm(values, gain):
    widened = values.astype(jnp.float32)
    inverse_rms = lax.rsqrt(jnp.mean(widened * widened, axis=-1, keepdims=True) + epsilon)
    return (widened * inverse_rms * gain).astype(jnp.bfloat16)


def slot_positions(route_block):
    picked_experts = route_block.reshape(route_block.shape[0] // MOE_DEV, MOE_DEV * TOP)
    onehot = (
        picked_experts[:, :, None] == jnp.arange(EXPERTS, dtype=jnp.int32)[None, None, :]
    ).astype(jnp.int32)
    before = jnp.cumsum(onehot, axis=1) - onehot
    return (picked_experts, jnp.sum(before * onehot, axis=2))


def one_table(slot_index, token_index):
    return jnp.full((EXPERTS * CAP,), -1, jnp.int32).at[slot_index].set(token_index)


def take_rows(normed, source):
    return jnp.take(normed, jnp.maximum(source, 0), axis=0)


def fill_slots(normed, picked_experts, positions):
    slot_index = picked_experts * CAP + positions
    token_index = jnp.broadcast_to(
        jnp.arange(MOE_DEV * TOP, dtype=jnp.int32) // TOP, slot_index.shape
    )
    source = jax.vmap(one_table)(slot_index, token_index)
    taken_rows = jax.vmap(take_rows)(normed, source)
    taken_rows = jnp.where((source >= 0)[:, :, None], taken_rows, jnp.zeros_like(taken_rows))
    return taken_rows.reshape(normed.shape[0], EXPERTS, CAP, normed.shape[2])


def on_device(
    conv_value,
    conv_gate,
    conv_taps,
    conv_gain,
    conv_bias,
    conv_projection,
    expert_input,
    expert_gain,
    route_experts,
    group_gate,
    expert_gate,
    gate_weight,
    up_weight,
    down_weight,
):
    gated_rows = (
        conv_value.astype(jnp.float32) * jax.nn.sigmoid(conv_gate.astype(jnp.float32))
    ).astype(jnp.bfloat16)
    reach_back = conv_taps.shape[0] - 1
    length = gated_rows.shape[0]
    earlier = passed_along(gated_rows[length - reach_back :], EP_TP, 1)
    extended = jnp.concatenate([earlier, gated_rows], axis=0)
    mixed_conv = jnp.zeros(gated_rows.shape, jnp.float32)
    for lag_step in range(reach_back + 1):
        window = lax.slice_in_dim(
            extended, reach_back - lag_step, reach_back - lag_step + length, axis=0
        )
        mixed_conv = mixed_conv + conv_taps[lag_step] * window.astype(jnp.float32)
    center = mixed_conv - jnp.mean(mixed_conv, axis=-1, keepdims=True)
    spread = jnp.mean(center * center, axis=-1, keepdims=True)
    activated = jax.nn.silu(center * lax.rsqrt(spread + epsilon) * conv_gain + conv_bias).astype(
        jnp.bfloat16
    )

    def project_rows(piece_rows, start_row):
        return jnp.dot(piece_rows, conv_projection, preferred_element_type=jnp.float32)

    conv_out = work_in_pieces(activated, "tp", 0, project_rows, 0).astype(jnp.bfloat16)
    quarters = lax.axis_size("tp")
    own_quarter = lax.axis_index("tp")
    picked_experts, positions = slot_positions(route_experts)
    own_rows = lax.dynamic_slice_in_dim(expert_input, own_quarter * MOE_DEV, MOE_DEV, 0)
    normed = root_mean_norm(own_rows, expert_gain)[None]
    own_experts = lax.dynamic_slice_in_dim(picked_experts, own_quarter, 1, 0)
    own_positions = lax.dynamic_slice_in_dim(positions, own_quarter, 1, 0)
    outgoing = fill_slots(normed, own_experts, own_positions)
    arrived = lax.all_to_all(outgoing, EP, split_axis=1, concat_axis=2, tiled=True)
    hidden_arrived = lax.all_gather(arrived, "tp", axis=0, tiled=True)
    gate_part = jnp.einsum(
        "qecd,edh->qech", hidden_arrived, gate_weight, preferred_element_type=jnp.float32
    )
    up_part = jnp.einsum(
        "qecd,edh->qech", hidden_arrived, up_weight, preferred_element_type=jnp.float32
    )
    hidden = (jax.nn.silu(gate_part) * up_part).astype(jnp.bfloat16)
    summed = jnp.einsum(
        "qech,ehd->qecd",
        lax.all_gather(hidden, "tp", axis=3, tiled=True),
        down_weight,
        preferred_element_type=jnp.float32,
    )
    returned = core_and_chips(summed.astype(jnp.bfloat16), (("ep_0", "ep_1"), "ep_2"), (1, 0), 2, 1)
    result_table = returned.reshape(quarters * EXPERTS * CAP, returned.shape[3])
    plane_index = jnp.arange(quarters, dtype=jnp.int32)[:, None]
    slot_index = (plane_index * EXPERTS + picked_experts) * CAP + positions
    picked = jnp.take(result_table, slot_index.reshape(-1), axis=0).reshape(
        -1, TOP, returned.shape[3]
    )
    route_share = group_gate[:, None] * expert_gate / jnp.sum(expert_gate, axis=1, keepdims=True)
    expert_out = jnp.sum(picked.astype(jnp.float32) * route_share[:, :, None], axis=1).astype(
        jnp.bfloat16
    )
    return (conv_out, expert_out)


def solution(mesh):
    finer = Mesh(mesh.devices.reshape(4, 4, 2, mesh.shape["tp"]), ("ep_0", "ep_1", "ep_2", "tp"))
    in_specs = (
        P(EP_TP, None),
        P(EP_TP, None),
        P(),
        P(),
        P(),
        P(None, "tp"),
        P(EP, None),
        P(),
        P(EP, None),
        P(EP),
        P(EP, None),
        P(EP, None, "tp"),
        P(EP, None, "tp"),
        P(EP, None, "tp"),
    )
    out_specs = (P(EP, "tp"), P(EP, "tp"))
    return jax.shard_map(
        on_device, mesh=finer, in_specs=in_specs, out_specs=out_specs, check_vma=False
    )
```

profile of v0, /device:TPU:1, one launch (start us, length us, event | category | flops | bytes accessed | tf_op | source)
XLA Modules:
  0.0 446.0 jit_solution(4297248506721945135)
XLA Ops:
  7.2 0.0 copy-start
  7.2 0.0 all-gather.7.cloned.1.call-start
  7.2 1.0 copy.56
  8.2 0.2 eq.29
  8.4 0.2 eq.25
  8.6 2.3 reduce-window.6
  10.9 0.1 slice.331
  11.0 0.1 copy.58
  11.1 0.1 fusion.65
  11.3 1.4 scatter_custom_fusion
  12.8 1.5 fusion.13
  14.3 0.1 broadcast_in_dim.62
  14.4 0.1 broadcast_in_dim.64
  14.5 1.6 fusion.62
  16.1 17.4 %gather_fusion.1 = bf16[512,4096]{1,0:T(8,128)(2,1)} fusion(bf16[1,128,4096]{2,1,0:T(8,128)(2,1)S(1)} %fusion.62, s32[512]{0:T(512)S(1)} %bitcast.161), kind=kCustom, calls=%fused_computation.1 | custom fusion | bytes 8392704 | tf_op jit(solution)/shard_map/vmap(jit(_take))/gather | solution.py:80
  33.5 2.6 select_select_fusion
  36.1 60.3 %all_to_all.22 = bf16[1,32,16,4096]{3,2,0,1:T(8,128)(2,1)} all-to-all(bf16[1,32,16,4096]{3,2,0,1:T(8,128)(2,1)S(1)} %select_select_fusion), channel_id=1, replica_groups=mesh['ep_0'=4,'ep_1'=4,'ep_2'=2,'tp'=4] {'ep_0','ep_1','ep_2'}, dimensions={1} | all-to-all | bytes 8388608 | tf_op jit(solution)/shard_map/all_to_all | solution.py:141
  96.3 0.0 all-gather.7.cloned.1.call-update
  96.3 0.2 all-gather.9.cloned.1.call-start
  96.6 151.2 %all-gather.7.cloned.1.call-done = bf16[4,1,512,4096]{3,2,1,0:T(8,128)(2,1)} async-done(((bf16[1,1,512,4096]{3,2,1,0:T(8,128)(2,1)}), bf16[4,1,512,4096]{3,2,1,0:T(8,128)(2,1)}) %all-gather.7.cloned.1.call-update) | async-done | bytes 16777232 | tf_op jit(solution)/shard_map/all_gather | solution.py:142
  247.8 8.9 %fusion = f32[4,512,256]{2,1,0:T(8,128)S(1)} fusion(bf16[4,1,512,4096]{3,2,1,0:T(8,128)(2,1)} %all-gather.7.cloned.1.call-done, bf16[1,4096,256]{2,1,0:T(8,128)(2,1)} %param.26), kind=kOutput, calls=%fused_computation.32 | convolution fusion | flops 4294967296 | bytes 20971520 | tf_op jit(solution)/shard_map/qecd,edh->qech/dot_general | solution.py:146
  256.7 2.3 copy-done.8
  258.9 0.6 copy-done.9
  259.5 6.0 %fusion.16 = bf16[4,1,512,256]{3,2,0,1:T(8,128)(2,1)} fusion(f32[4,512,256]{2,1,0:T(8,128)S(1)} %fusion, bf16[1,4096,256]{2,1,0:T(8,128)(2,1)S(1)} %copy-done.9, bf16[4,1,512,4096]{3,2,1,0:T(8,128)(2,1)S(1)} %copy-done.8), kind=kOutput, calls=%fused_computation.57 | convolution fusion | flops 4298113024 | bytes 22020096 | tf_op jit(solution)/shard_map/qecd,edh->qech/dot_general | solution.py:143
  265.5 0.0 all-gather.9.cloned.1.call-update
  265.6 0.0 all-gather.11.cloned.1.call-start
  265.6 2.8 multiply_convert_fusion.1
  268.4 3.1 collective-permute-start
  271.5 0.0 copy-done.2
  271.6 0.1 fusion.77
  271.7 0.1 fusion.78
  271.8 4.5 %collective-permute-done = bf16[30,2048]{1,0:T(8,128)(2,1)S(1)} collective-permute-done((bf16[30,2048]{1,0:T(8,128)(2,1)S(1)}, bf16[30,2048]{1,0:T(8,128)(2,1)S(1)}, u32[]{:S(2)}, u32[]{:S(2)}) %collective-permute-start) | collective-permute-done | bytes 122912 | tf_op jit(solution)/shard_map/ppermute | solution.py:21
  276.3 14.3 %fusion.75 = (f32[384]{0:T(512)S(1)}, f32[384,2048]{1,0:T(8,128)S(1)}) fusion(bf16[384,2048]{1,0:T(8,128)(2,1)S(1)} %multiply_convert_fusion.1, bf16[30,2048]{1,0:T(8,128)(2,1)S(1)} %collective-permute-done, f32[2048]{0:T(1024)S(1)} %bitcast.198, f32[2048]{0:T(1024)S(1)} %bitcast.199, f32[2048]{0:T(1024)S(1)} %bitcast.170, f32[2048]{0:T(1024)S(1)} %bitcast.171, ...), kind=kLoop, calls=%fused_computation.145 | loop fusion | flops 143916672 | bytes 5096960 | tf_op jit(solution)/shard_map/reduce_sum | solution.py:123
  290.6 0.5 multiply_reduce_fusion.1
  291.1 1.3 multiply_convert_fusion
  292.4 1.3 fusion.76
  293.6 0.0 all-gather.11.cloned.1.call-update
  293.6 0.3 all-gather.13.cloned.1.call-start
  293.9 0.3 all-gather.13.cloned.1.call-update
  294.2 22.6 %all-gather.9.cloned.1.call-done = bf16[4,1,512,1024]{3,2,0,1:T(8,128)(2,1)} async-done(((bf16[4,1,512,256]{3,2,0,1:T(8,128)(2,1)}), bf16[4,1,512,1024]{3,2,0,1:T(8,128)(2,1)}) %all-gather.9.cloned.1.call-update) | async-done | bytes 4194320 | tf_op jit(solution)/shard_map/all_gather | solution.py:152
  316.8 6.9 %fusion.10 = bf16[4,512,1024]{2,1,0:T(8,128)(2,1)S(1)} fusion(bf16[4,1,512,1024]{3,2,0,1:T(8,128)(2,1)} %all-gather.9.cloned.1.call-done, bf16[1,1024,1024]{2,1,0:T(8,128)(2,1)S(1)} %copy-done), kind=kOutput, calls=%fused_computation.50 | convolution fusion | flops 4297064448 | bytes 10485760 | tf_op jit(solution)/shard_map/qech,ehd->qecd/dot_general | solution.py:150
  323.8 0.8 copy.64
  324.6 0.8 copy.65
  325.4 8.8 %all_to_all.23 = bf16[16,2,4,1,16,1024]{5,4,0,2,3,1:T(8,128)(2,1)S(1)} all-to-all(bf16[16,2,4,1,16,1024]{5,4,0,2,3,1:T(8,128)(2,1)S(1)} %copy.65), channel_id=1, replica_groups=mesh['ep_0'=4,'ep_1'=4,'ep_2'=2,'tp'=4] {'ep_2'}, dimensions={1} | all-to-all | bytes 8388608 | tf_op jit(solution)/shard_map/all_to_all | solution.py:50
  334.2 2.4 copy.66
  336.6 6.9 %all-to-all-start.2 = ((bf16[16,2,4,1,16,1024]{5,4,1,2,3,0:T(8,128)(2,1)}), bf16[16,2,4,1,16,1024]{5,4,1,2,3,0:T(8,128)(2,1)}, u32[]{:S(2)}, u32[]{:S(2)}) async-start(bf16[16,2,4,1,16,1024]{5,4,1,2,3,0:T(8,128)(2,1)} %copy.66), calls=%async_computation.2 | async-start | bytes 8388608 | tf_op jit(solution)/shard_map/all_to_all | solution.py:50
  343.5 0.2 reshape.234
  343.7 0.2 reduce_sum.61
  343.9 0.1 broadcast_bitcast_fusion
  344.0 0.1 copy.61
  344.1 0.1 broadcast_bitcast_fusion.1
  344.2 0.2 copy.62
  344.5 0.1 copy.70
  344.6 16.0 %all-gather.11.cloned.1.call-done = bf16[768,2048]{1,0:T(8,128)(2,1)} async-done(((bf16[192,2048]{1,0:T(8,128)(2,1)}), bf16[768,2048]{1,0:T(8,128)(2,1)}) %all-gather.11.cloned.1.call-update) | async-done | bytes 3145744 | tf_op jit(solution)/shard_map/all_gather | solution.py:37
  360.6 6.6 %fusion.23 = bf16[4,192,1024]{2,1,0:T(8,128)(2,1)S(1)} fusion(bf16[4,192,2048]{2,1,0:T(8,128)(2,1)} %bitcast.205, bf16[2048,1024]{1,0:T(8,128)(2,1)} %param.19), kind=kOutput, calls=%fused_computation.66 | convolution fusion | flops 3222011904 | bytes 8912896 | tf_op jit(solution)/shard_map/vmap()/dot_general | solution.py:130
  367.2 34.6 %all-gather.13.cloned.1.call-done = bf16[768,2048]{1,0:T(8,128)(2,1)} async-done(((bf16[192,2048]{1,0:T(8,128)(2,1)}), bf16[768,2048]{1,0:T(8,128)(2,1)}) %all-gather.13.cloned.1.call-update) | async-done | bytes 3145744 | tf_op jit(solution)/shard_map/all_gather | solution.py:37
  401.8 6.6 %fusion.26 = bf16[4,192,1024]{2,1,0:T(8,128)(2,1)S(1)} fusion(bf16[4,192,2048]{2,1,0:T(8,128)(2,1)} %bitcast.206, bf16[2048,1024]{1,0:T(8,128)(2,1)} %param.19), kind=kOutput, calls=%fused_computation.67 | convolution fusion | flops 3222011904 | bytes 8912896 | tf_op jit(solution)/shard_map/vmap()/dot_general | solution.py:130
  408.4 2.0 pad_maximum_fusion
  410.4 0.0 all-to-all-done.2
  410.4 2.6 copy.67
  413.0 2.4 copy.68
  415.4 8.9 %gather_fusion = bf16[1024,1024]{1,0:T(8,128)(2,1)} fusion(bf16[2048,1024]{1,0:T(8,128)(2,1)} %bitcast.160, s32[1024]{0:T(1024)S(1)} %broadcast_clamp_fusion), kind=kCustom, calls=%fused_computation | custom fusion | bytes 4198400 | tf_op jit(solution)/shard_map/jit(_take)/gather | solution.py:160
  424.3 4.1 gather.15
  428.4 11.0 %multiply_reduce_fusion = bf16[512,1024]{1,0:T(8,128)(2,1)} fusion(bf16[512,2,1024]{2,1,0:T(2,128)(2,1)} %gather.15, pred[512,2]{1,0:T(8,128)(4,1)S(1)} %copy.62, f32[512,2]{1,0:T(8,128)S(1)} %copy.70), kind=kLoop, calls=%fused_computation.42 | loop fusion | flops 3670016 | bytes 3150848 | tf_op jit(solution)/shard_map/reduce_sum | solution.py:164
  (40 shorter events, 0.3 us)
Async XLA Ops:
  7.2 309.7 %copy-start = (bf16[1,1024,1024]{2,1,0:T(8,128)(2,1)S(1)}, bf16[1,1024,1024]{2,1,0:T(8,128)(2,1)}, u32[]{:S(2)}) copy-start(bf16[1,1024,1024]{2,1,0:T(8,128)(2,1)} %param.27) | copy-start | bytes 6291460
  7.2 240.6 %all-gather.7.cloned.1.call-start = ((), (), s32[]{:S(2)}) async-start(), calls=%async_computation.3 | async-start | bytes 20971520 | tf_op jit(solution)/shard_map/all_gather | solution.py:142
  96.3 220.5 %all-gather.9.cloned.1.call-start = ((), (), s32[]{:S(2)}) async-start(), calls=%async_computation.4 | async-start | bytes 5242880 | tf_op jit(solution)/shard_map/all_gather | solution.py:152
  247.8 11.1 %copy-start.8 = (bf16[4,1,512,4096]{3,2,1,0:T(8,128)(2,1)S(1)}, bf16[4,1,512,4096]{3,2,1,0:T(8,128)(2,1)}, u32[]{:S(2)}) copy-start(bf16[4,1,512,4096]{3,2,1,0:T(8,128)(2,1)} %all-gather.7.cloned.1.call-done) | copy-start | bytes 50331652
  247.8 11.7 %copy-start.9 = (bf16[1,4096,256]{2,1,0:T(8,128)(2,1)S(1)}, bf16[1,4096,256]{2,1,0:T(8,128)(2,1)}, u32[]{:S(2)}) copy-start(bf16[1,4096,256]{2,1,0:T(8,128)(2,1)} %param.25) | copy-start | bytes 6291460
  265.5 6.0 %copy-start.2 = (f32[31,2048]{1,0:T(8,128)S(1)}, f32[31,2048]{1,0:T(8,128)}, u32[]{:S(2)}) copy-start(f32[31,2048]{1,0:T(8,128)} %param.16) | copy-start | bytes 761860
  265.6 95.1 %all-gather.11.cloned.1.call-start = ((), (), s32[]{:S(2)}) async-start(), calls=%async_computation.5 | async-start | bytes 3932160 | tf_op jit(solution)/shard_map/all_gather | solution.py:37
  268.4 7.8 %collective-permute-start = (bf16[30,2048]{1,0:T(8,128)(2,1)S(1)}, bf16[30,2048]{1,0:T(8,128)(2,1)S(1)}, u32[]{:S(2)}, u32[]{:S(2)}) collective-permute-start(bf16[30,2048]{1,0:T(8,128)(2,1)S(1)} %slice.270), channel_id=1, source_target_pairs={{0,1},{1,2},{2,3},{3,4},{4,5},{5,6},{6,7},{7,8},{8,9},{9,10},{10,1... | collective-permute-start | bytes 368648 | tf_op jit(solution)/shard_map/ppermute | solution.py:21
  276.3 14.8 %copy-start.5 = (f32[2048]{0:T(1024)S(1)}, f32[2048]{0:T(1024)}, u32[]{:S(2)}) copy-start(f32[2048]{0:T(1024)} %param.18) | copy-start | bytes 24580
  276.3 14.8 %copy-start.6 = (f32[2048]{0:T(1024)S(1)}, f32[2048]{0:T(1024)}, u32[]{:S(2)}) copy-start(f32[2048]{0:T(1024)} %param.17) | copy-start | bytes 24580
  293.6 108.2 %all-gather.13.cloned.1.call-start = ((), (), s32[]{:S(2)}) async-start(), calls=%async_computation.6 | async-start | bytes 3932160 | tf_op jit(solution)/shard_map/all_gather | solution.py:37
  336.6 7.6 %copy-start.3 = (s32[512,2]{0,1:T(2,128)S(1)}, s32[512,2]{0,1:T(2,128)}, u32[]{:S(2)}) copy-start(s32[512,2]{0,1:T(2,128)} %param.22) | copy-start | bytes 12292
  336.6 7.8 %copy-start.4 = (f32[512,2]{0,1:T(2,128)S(1)}, f32[512,2]{0,1:T(2,128)}, u32[]{:S(2)}) copy-start(f32[512,2]{0,1:T(2,128)} %param.24) | copy-start | bytes 12292
  336.6 7.8 %copy-start.7 = (f32[512]{0:T(512)S(1)}, f32[512]{0:T(512)}, u32[]{:S(2)}) copy-start(f32[512]{0:T(512)} %param.23) | copy-start | bytes 6148
  336.6 73.8 %all-to-all-start.2 = ((bf16[16,2,4,1,16,1024]{5,4,1,2,3,0:T(8,128)(2,1)}), bf16[16,2,4,1,16,1024]{5,4,1,2,3,0:T(8,128)(2,1)}, u32[]{:S(2)}, u32[]{:S(2)}) async-start(bf16[16,2,4,1,16,1024]{5,4,1,2,3,0:T(8,128)(2,1)} %copy.66), calls=%async_computation.2 | async-start | bytes 8388608 | tf_op jit(solution)/shard_map/all_to_all | solution.py:50
  415.4 24.1 %copy-start.1 = (bf16[1,1024,1024]{2,1,0:T(8,128)(2,1)S(1)}, bf16[1,1024,1024]{2,1,0:T(8,128)(2,1)}, u32[]{:S(2)}) copy-start(bf16[1,1024,1024]{2,1,0:T(8,128)(2,1)} %param.27) | copy-start | bytes 6291460
Sparse Core Ops, SparseCore 0:
  96.5 151.2 all-gather.6
  265.7 51.1 all-gather.8
  319.1 41.5 all-gather.10
  362.2 39.6 all-gather.12
where the time goes:
time: 447 us; the launch traced here: 446 us
  waiting for transfers between devices  229 us (51%)
  blocking collectives  69 us (15%)
  local copies, waits for them, and re-layouts  47.9 us (11%)
  other arithmetic  40.1 us (9%)
  matrix products  34.9 us (8%)
  between operations  14.1 us (3%)
  starting transfers between devices  10.5 us (2%)
    all_gather x1, waiting for transfers between devices, on_device(): hidden_arrived = lax.all_gather(arrived, 'tp', axis=0, tiled=True)  151 us
    all_to_all x1, blocking collectives, on_device(): lax.all_to_all(outgoing, EP, split_axis=1, concat_axis=2, tiled=True)  60.3 us
    all_gather x2, waiting for transfers between devices, work_in_pieces(): outs.append(jax.vmap(apply)(lax.all_gather(section, axis), starts))  50.6 us
    all_gather x1, waiting for transfers between devices, on_device(): lax.all_gather(hidden, 'tp', axis=3, tiled=True)  22.6 us
    gather x2, local copies, waits for them, and re-layouts, take_rows(): return jnp.take(normed, jnp.maximum(source, 0), axis=0)  17.4 us
    reduce_sum x1, other arithmetic, on_device(): center = mixed_conv - jnp.mean(mixed_conv, axis=-1, keepdims=True)  14.3 us
    dot_general x2, matrix products, project_rows(): jnp.dot(piece_rows, conv_projection, preferred_element_type=jnp.float32)  13.1 us
    gather x2, local copies, waits for them, and re-layouts, on_device(): jnp.take(result_table, slot_index.reshape(-1), axis=0)  13 us
  transfers between devices with their start and end apart: 6, of which 5 were waited for; matrix products, arithmetic and copies ran while one was open for 11% of the time, Pallas kernels for 0%

commit v1 on v0

v1 whole, which is shorter than its diff:
```python
import jax
import jax.numpy as jnp
from jax import lax
from jax.experimental import pallas as pl
from jax.experimental.pallas import tpu as pltpu
from jax.sharding import PartitionSpec as P

EXPERTS = 32
TOP = 2
MOE_DEV = 128
CAP = 16
D = 4096
HID_PART = 256
OUT_PART = 1024
EP_TP = ("ep", "tp")
MESH = pl.DeviceIdType.MESH
BF16 = jnp.bfloat16
F32 = jnp.float32

epsilon = 1e-06


def expert_kernel(
    rows_hbm,
    gain,
    route,
    share,
    gate_hbm,
    up_hbm,
    down_hbm,
    out,
    tokens,
    slots,
    arrived,
    w_gate,
    w_up,
    w_down,
    hidden,
    result,
    back,
    partial,
    landed,
    meta,
    acc_gate,
    acc_up,
    load_sem,
    z_send,
    z_recv,
    m_send,
    m_recv,
    y_send,
    y_recv,
    x_send,
    x_recv,
    h_send,
    h_recv,
    b_send,
    b_recv,
    p_send,
    p_recv,
):
    ep = lax.axis_index("ep")
    x = lax.axis_index("tp")
    z, y, c = ep // 8, (ep // 2) % 4, ep % 2

    def at(dz, dy, dc, dx):
        there = (((z + dz) % 4) * 4 + (y + dy) % 4) * 2 + (c + dc) % 2
        return (there, (x + dx) % 4)

    def remote(src, dst, send, recv, device):
        return pltpu.make_async_remote_copy(
            src_ref=src, dst_ref=dst, send_sem=send, recv_sem=recv, device_id=device, device_id_type=MESH
        )

    quarter = (x, (x + 1) % 4)

    raw = [
        pltpu.make_async_copy(
            rows_hbm.at[pl.ds(pl.multiple_of(quarter[i] * MOE_DEV, MOE_DEV), MOE_DEV)],
            slots.at[2, i],
            load_sem.at[i],
        )
        for i in range(2)
    ]
    weights = [
        pltpu.make_async_copy(gate_hbm.at[0], w_gate, load_sem.at[2]),
        pltpu.make_async_copy(up_hbm.at[0], w_up, load_sem.at[3]),
        pltpu.make_async_copy(down_hbm.at[0], w_down, load_sem.at[4]),
    ]
    for load in raw + weights:
        load.start()

    barrier = pltpu.get_barrier_semaphore()
    partners = [at(dz, 0, 0, 0) for dz in (1, 2, 3)]
    partners += [at(0, dy, dc, 0) for dy in range(4) for dc in range(2) if dy or dc]
    partners += [at(0, 0, 0, dx) for dx in (1, 2, 3)]
    for device in partners:
        pl.semaphore_signal(barrier, inc=1, device_id=device, device_id_type=MESH)

    lane = lax.broadcasted_iota(jnp.int32, (128, 128), 1)
    sub = lax.broadcasted_iota(jnp.int32, (128, 128), 0)
    earlier = jnp.where(sub < lane, 1.0, 0.0).astype(BF16)
    expert_row = lax.broadcasted_iota(jnp.int32, (EXPERTS, 128), 0)
    for q in range(4):
        first, second = route[q, 0:1, :], route[q, 1:2, :]
        hot0 = jnp.where(expert_row == first, 1.0, 0.0)
        hot1 = jnp.where(expert_row == second, 1.0, 0.0)
        before = jnp.dot((hot0 + hot1).astype(BF16), earlier, preferred_element_type=F32)
        pos0 = jnp.sum(before * hot0, axis=0, keepdims=True)
        pos1 = jnp.sum(before * hot1, axis=0, keepdims=True)
        meta[0, q, 0:1, :] = first.astype(F32) * CAP + pos0
        meta[0, q, 1:2, :] = second.astype(F32) * CAP + pos1
        meta[0, q, 2:4, :] = share[q]
        meta[0, q, 4:8, :] = jnp.zeros((4, 128), F32)

    for i in range(2):
        raw[i].wait()

        @pl.loop(0, 8)
        def _(t):
            r = pl.ds(pl.multiple_of(t * 16, 16), 16)
            wide = slots[2, i, r, :].astype(F32)
            inverse = lax.rsqrt(jnp.mean(wide * wide, axis=-1, keepdims=True) + epsilon)
            tokens[0, i, r, :] = (wide * inverse * gain[...]).astype(BF16)

    pl.semaphore_wait(barrier, len(partners))

    meta_copies = {
        dz: remote(meta.at[0], meta.at[dz], m_send.at[dz], m_recv.at[dz], at(dz, 0, 0, 0)) for dz in (1, 2, 3)
    }
    for dz in (1, 3, 2):
        meta_copies[dz].start()

    def z_copy(dz, i):
        if dz == 2:
            source, step = (1, 1) if i == 0 else (3, 3)
        else:
            source, step = 0, dz
        return remote(tokens.at[source, i], tokens.at[dz, i], z_send.at[dz, i], z_recv.at[dz, i], at(step, 0, 0, 0))

    for dz, i in ((1, 0), (3, 1), (1, 1), (3, 0)):
        z_copy(dz, i).start()

    plane = (z * 128).astype(F32)
    slot_row = lax.broadcasted_iota(jnp.int32, (128, 128), 0).astype(F32)

    def y_copy(dz, i, dy, dc):
        there = ((y + dy) % 4) * 2 + (c + dc) % 2
        k = dy * 2 + dc
        return remote(
            slots.at[dz, i, pl.ds(pl.multiple_of(there * CAP, CAP), CAP)],
            arrived.at[dz, k, quarter[i]],
            y_send.at[dz, i, k],
            y_recv.at[dz, i, k],
            at(0, dy, dc, 0),
        )

    y_order = [(0, 1), (1, 0), (3, 0), (1, 1), (3, 1), (2, 0), (2, 1)]

    def build(dz, i):
        q = quarter[i]
        hot = jnp.where(slot_row == meta[dz, q, 0:1, :] - plane, 1.0, 0.0)
        hot = hot + jnp.where(slot_row == meta[dz, q, 1:2, :] - plane, 1.0, 0.0)
        hot = hot.astype(BF16)

        @pl.loop(0, D // 512)
        def _(t):
            cols = pl.ds(pl.multiple_of(t * 512, 512), 512)
            slots[dz, i, :, cols] = jnp.dot(hot, tokens[dz, i, :, cols], preferred_element_type=F32).astype(BF16)

        for dy, dc in y_order:
            y_copy(dz, i, dy, dc).start()
        own = pl.ds(pl.multiple_of((y * 2 + c) * CAP, CAP), CAP)
        arrived[dz, 0, q] = slots[dz, i, own, :]

    def take_z(dz, i):
        z_copy(dz, i).wait_recv()

    def x_copy(dz, i, k):
        q = quarter[i]
        return remote(
            arrived.at[dz, k, q],
            arrived.at[dz, k, q],
            x_send.at[dz, i, k],
            x_recv.at[dz, i, k],
            at(0, 0, 0, 1 if i == 0 else 3),
        )

    def pass_on(dz, i):
        x_copy(dz, i, 0).start()
        for dy, dc in y_order:
            y_copy(dz, i, dy, dc).wait_recv()
            x_copy(dz, i, dy * 2 + dc).start()

    def x_landing(dz, i, k):
        q = (x + 3) % 4 if i == 0 else (x + 2) % 4
        return remote(
            arrived.at[dz, k, q],
            arrived.at[dz, k, q],
            x_send.at[dz, i, k],
            x_recv.at[dz, i, k],
            at(0, 0, 0, 3 if i == 0 else 1),
        )

    def h_copy(dz, dx):
        return remote(hidden.at[dz, x], hidden.at[dz, x], h_send.at[dz, dx], h_recv.at[dz, dx], at(0, 0, 0, dx))

    def h_landing(dz, dx):
        source = (x + 4 - dx) % 4
        return remote(
            hidden.at[dz, source], hidden.at[dz, source], h_send.at[dz, dx], h_recv.at[dz, dx], at(0, 0, 0, dx)
        )

    KB = 512

    def first_product(g):
        for i in range(2):
            for k in range(8):
                x_landing(g, i, k).wait_recv()
        acc_gate[...] = jnp.zeros_like(acc_gate)
        acc_up[...] = jnp.zeros_like(acc_up)

        @pl.loop(0, D // KB)
        def _(t):
            cols = pl.ds(pl.multiple_of(t * KB, KB), KB)
            piece = arrived[g, :, :, :, cols].reshape(512, KB)
            acc_gate[...] += jnp.dot(piece, w_gate[cols, :], preferred_element_type=F32)
            acc_up[...] += jnp.dot(piece, w_up[cols, :], preferred_element_type=F32)

        @pl.loop(0, 8)
        def _(t):
            r = pl.ds(pl.multiple_of(t * 64, 64), 64)
            gate = acc_gate[r, :]
            hidden[g, x, r, :] = (gate / (1.0 + jnp.exp(-gate)) * acc_up[r, :]).astype(BF16)

        for dx in (1, 3, 2):
            h_copy(g, dx).start()

    def b_copy(g, dy, dc):
        k = dy * 2 + dc
        return remote(
            result.at[g, k],
            back.at[g, :, y * 2 + c],
            b_send.at[g, k],
            b_recv.at[g, k],
            at(0, (4 - dy) % 4, dc, 0),
        )

    def b_landing(g, dy, dc):
        k = dy * 2 + dc
        source = ((y + dy) % 4) * 2 + (c + dc) % 2
        return remote(
            result.at[g, k],
            back.at[g, :, source],
            b_send.at[g, k],
            b_recv.at[g, k],
            at(0, (4 - dy) % 4, dc, 0),
        )

    def second_product(g):
        for dx in (1, 3, 2):
            h_landing(g, dx).wait_recv()

        @pl.loop(0, OUT_PART // 256)
        def _(t):
            cols = pl.ds(pl.multiple_of(t * 256, 256), 256)
            total = jnp.dot(hidden[g, 0], w_down[0:256, cols], preferred_element_type=F32)
            for s in range(1, 4):
                total += jnp.dot(hidden[g, s], w_down[s * 256 : (s + 1) * 256, cols], preferred_element_type=F32)
            result[g, :, :, :, cols] = total.astype(BF16).reshape(8, 4, CAP, 256)

        for dy, dc in y_order:
            b_copy(g, dy, dc).start()
        back[g, :, y * 2 + c] = result[g, 0]

    def p_copy(g):
        return remote(partial.at[g], landed.at[g - 1], p_send.at[g], p_recv.at[g], at(4 - g, 0, 0, 0))

    def combine(g):
        for dy, dc in y_order:
            b_landing(g, dy, dc).wait_recv()

        @pl.loop(0, 4)
        def _(q):
            weight = jnp.where(slot_row == meta[g, q, 0:1, :] - plane, meta[g, q, 2:3, :], 0.0)
            weight = weight + jnp.where(slot_row == meta[g, q, 1:2, :] - plane, meta[g, q, 3:4, :], 0.0)
            high = weight.astype(BF16)
            low = (weight - high.astype(F32)).astype(BF16)
            rows = back[g, q].reshape(128, OUT_PART)
            dims = (((0,), (0,)), ((), ()))
            total = lax.dot_general(high, rows, dims, preferred_element_type=F32)
            total += lax.dot_general(low, rows, dims, preferred_element_type=F32)
            partial[g, pl.ds(pl.multiple_of(q * 128, 128), 128), :] = total.astype(BF16)

        if g:
            p_copy(g).start()

    build(0, 0)
    build(0, 1)
    pass_on(0, 0)
    pass_on(0, 1)
    for load in weights:
        load.wait()
    meta_copies[1].wait_recv()
    meta_copies[3].wait_recv()
    take_z(1, 0)
    z_copy(2, 0).start()
    build(1, 0)
    take_z(3, 1)
    z_copy(2, 1).start()
    build(3, 1)
    pass_on(1, 0)
    pass_on(3, 1)
    first_product(0)
    take_z(1, 1)
    build(1, 1)
    take_z(3, 0)
    build(3, 0)
    pass_on(1, 1)
    pass_on(3, 0)
    second_product(0)
    meta_copies[2].wait_recv()
    take_z(2, 0)
    build(2, 0)
    take_z(2, 1)
    build(2, 1)
    first_product(1)
    pass_on(2, 0)
    pass_on(2, 1)
    first_product(3)
    second_product(1)
    combine(0)
    second_product(3)
    first_product(2)
    combine(1)
    combine(3)
    second_product(2)
    combine(2)

    for g in (1, 3, 2):
        p_copy(g).wait_recv()

    @pl.loop(0, 16)
    def _(t):
        r = pl.ds(pl.multiple_of(t * 32, 32), 32)
        total = partial[0, r, :].astype(F32) + landed[0, r, :].astype(F32)
        total = total + landed[1, r, :].astype(F32) + landed[2, r, :].astype(F32)
        out[r, :] = total.astype(BF16)

    for dz in (1, 2, 3):
        meta_copies[dz].wait_send()
        p_copy(dz).wait_send()
        for i in range(2):
            z_copy(dz, i).wait_send()
    for g in range(4):
        for dx in (1, 2, 3):
            h_copy(g, dx).wait_send()
        for dy, dc in y_order:
            b_copy(g, dy, dc).wait_send()
        for i in range(2):
            for k in range(8):
                x_copy(g, i, k).wait_send()
            for dy, dc in y_order:
                y_copy(g, i, dy, dc).wait_send()


def expert_branch(expert_input, expert_gain, route, share, gate_weight, up_weight, down_weight):
    vmem, hbm = pl.BlockSpec(memory_space=pltpu.VMEM), pl.BlockSpec(memory_space=pl.ANY)
    dma = pltpu.SemaphoreType.DMA
    return pl.pallas_call(
        expert_kernel,
        name="experts",
        out_shape=jax.ShapeDtypeStruct((512, OUT_PART), BF16),
        in_specs=[hbm, vmem, vmem, vmem, hbm, hbm, hbm],
        out_specs=vmem,
        scratch_shapes=[
            pltpu.VMEM((4, 2, 128, D), BF16),
            pltpu.VMEM((4, 2, 128, D), BF16),
            pltpu.VMEM((4, 8, 4, CAP, D), BF16),
            pltpu.VMEM((D, HID_PART), BF16),
            pltpu.VMEM((D, HID_PART), BF16),
            pltpu.VMEM((1024, OUT_PART), BF16),
            pltpu.VMEM((4, 4, 512, HID_PART), BF16),
            pltpu.VMEM((4, 8, 4, CAP, OUT_PART), BF16),
            pltpu.VMEM((4, 4, 8, CAP, OUT_PART), BF16),
            pltpu.VMEM((4, 512, OUT_PART), BF16),
            pltpu.VMEM((3, 512, OUT_PART), BF16),
            pltpu.VMEM((4, 4, 8, 128), F32),
            pltpu.VMEM((512, HID_PART), F32),
            pltpu.VMEM((512, HID_PART), F32),
            dma((5,)),
            dma((4, 2)),
            dma((4, 2)),
            dma((4,)),
            dma((4,)),
            dma((4, 2, 8)),
            dma((4, 2, 8)),
            dma((4, 2, 8)),
            dma((4, 2, 8)),
            dma((4, 4)),
            dma((4, 4)),
            dma((4, 8)),
            dma((4, 8)),
            dma((4,)),
            dma((4,)),
        ],
        compiler_params=pltpu.CompilerParams(
            collective_id=0, has_side_effects=True, vmem_limit_bytes=67_043_328
        ),
        cost_estimate=pl.CostEstimate(flops=150_000_000_000, bytes_accessed=16 << 20, transcendentals=0),
    )(expert_input, expert_gain, route, share, gate_weight, up_weight, down_weight)


def on_device(
    conv_value,
    conv_gate,
    conv_taps,
    conv_gain,
    conv_bias,
    conv_projection,
    expert_input,
    expert_gain,
    route_experts,
    group_gate,
    expert_gate,
    gate_weight,
    up_weight,
    down_weight,
):
    gated_rows = (
        conv_value.astype(jnp.float32) * jax.nn.sigmoid(conv_gate.astype(jnp.float32))
    ).astype(jnp.bfloat16)
    reach_back = conv_taps.shape[0] - 1
    length = gated_rows.shape[0]
    count = lax.axis_size(EP_TP)
    earlier = lax.ppermute(gated_rows[length - reach_back :], EP_TP, [(s, s + 1) for s in range(count - 1)])
    extended = jnp.concatenate([earlier, gated_rows], axis=0)
    mixed_conv = jnp.zeros(gated_rows.shape, jnp.float32)
    for lag_step in range(reach_back + 1):
        window = lax.slice_in_dim(
            extended, reach_back - lag_step, reach_back - lag_step + length, axis=0
        )
        mixed_conv = mixed_conv + conv_taps[lag_step] * window.astype(jnp.float32)
    center = mixed_conv - jnp.mean(mixed_conv, axis=-1, keepdims=True)
    spread = jnp.mean(center * center, axis=-1, keepdims=True)
    activated = jax.nn.silu(center * lax.rsqrt(spread + epsilon) * conv_gain + conv_bias).astype(
        jnp.bfloat16
    )

    route_share = group_gate[:, None] * expert_gate / jnp.sum(expert_gate, axis=1, keepdims=True)
    route = route_experts.reshape(4, MOE_DEV, TOP).transpose(0, 2, 1)
    share = route_share.reshape(4, MOE_DEV, TOP).transpose(0, 2, 1)
    activated, route, share = lax.optimization_barrier((activated, route, share))
    gathered = lax.all_gather(activated, "tp", axis=0, tiled=True)
    expert_out = expert_branch(
        expert_input, expert_gain[None], route, share, gate_weight, up_weight, down_weight
    )
    conv_out = jnp.dot(gathered, conv_projection, preferred_element_type=jnp.float32).astype(jnp.bfloat16)
    return (conv_out, expert_out)


def solution(mesh):
    in_specs = (
        P(EP_TP, None),
        P(EP_TP, None),
        P(),
        P(),
        P(),
        P(None, "tp"),
        P("ep", None),
        P(),
        P("ep", None),
        P("ep"),
        P("ep", None),
        P("ep", None, "tp"),
        P("ep", None, "tp"),
        P("ep", None, "tp"),
    )
    out_specs = (P("ep", "tp"), P("ep", "tp"))
    return jax.shard_map(
        on_device, mesh=mesh, in_specs=in_specs, out_specs=out_specs, check_vma=False
    )
```

time: 447 us -> 326 us (0.73)
  Pallas kernels: 0 us -> 270 us
  waiting for transfers between devices: 229 us -> 4.15 us
  blocking collectives: 69 us -> 0 us
  local copies, waits for them, and re-layouts: 47.9 us -> 1.21 us
  matrix products: 34.9 us -> 11.2 us
  other arithmetic: 40.1 us -> 20.6 us
  starting transfers between devices: 10.5 us -> 3.97 us
    pallas_call x0 -> x1, Pallas kernels: none -> 270 us  [expert_branch(): pl.pallas_call(expert_kernel, name='experts', out_shape=jax.ShapeDtypeStr...]
    all_gather x4 -> x1, waiting for transfers between devices: 224 us -> 0.02 us  [on_device(): gathered = lax.all_gather(activated, 'tp', axis=0, tiled=True)]
    all_to_all x2 -> x0, blocking collectives: 69 us -> none  [the longest x1 60.3 us: on_device(): lax.all_to_all(outgoing, EP, split_axis=1, concat_axis=2, tiled=True)]
    gather x4 -> x0, local copies, waits for them, and re-layouts: 30.4 us -> none  [the longest x2 17.4 us: take_rows(): return jnp.take(normed, jnp.maximum(source, 0), axis=0)]
    dot_general x5 -> x1, matrix products: 34.9 us -> 11.2 us  [on_device(): jnp.dot(gathered, conv_projection, preferred_element_type=jnp.float32)]
    reduce_sum x3 -> x0, other arithmetic: 12.7 us -> none  [the longest x1 11 us: on_device(): jnp.sum(picked.astype(jnp.float32) * route_share[:, :, None], axis=1)]
    all_to_all x1 -> x0, starting transfers between devices: 6.88 us -> none  [exchange_in_order(): lax.all_to_all(blocks, axes[k], split_axis=k, concat_axis=k, tiled=True)]
    all_to_all x2 -> x0, local copies, waits for them, and re-layouts: 5.03 us -> none  [exchange_in_order(): lax.all_to_all(blocks, axes[k], split_axis=k, concat_axis=k, tiled=True)]
  transfers between devices with their start and end apart: 6 -> 2, of which waited for: 5 -> 1; matrix products, arithmetic and copies ran while one was open for 11% -> 0% of each run, Pallas kernels for 0% -> 83%
where the time goes in v1:
time: 326 us
  Pallas kernels  270 us (83%)
  other arithmetic  20.6 us (6%)
  between operations  14.2 us (4%)
  matrix products  11.2 us (3%)
  waiting for transfers between devices  4.15 us (1%)
  starting transfers between devices  3.97 us (1%)
    pallas_call x1, Pallas kernels, expert_branch(): pl.pallas_call(expert_kernel, name='experts', out_shape=jax.ShapeDtypeStr...  270 us
    reduce_sum x1, other arithmetic, on_device(): center = mixed_conv - jnp.mean(mixed_conv, axis=-1, keepdims=True)  14.3 us
    dot_general x1, matrix products, on_device(): jnp.dot(gathered, conv_projection, preferred_element_type=jnp.float32)  11.2 us
  transfers between devices with their start and end apart: 2, of which 1 were waited for; matrix products, arithmetic and copies ran while one was open for 0% of the time, Pallas kernels for 83%

profile of v1, /device:TPU:1, one launch (start us, length us, event | category | flops | bytes accessed | tf_op | source)
XLA Modules:
  0.0 325.7 jit_solution(10816924395269457128)
XLA Ops:
  7.2 0.0 copy-start.1
  7.2 0.0 copy-start.2
  7.2 0.0 copy-start.5
  7.2 0.0 all-gather.2.cloned.1.call-start
  7.2 2.8 multiply_convert_fusion.1
  10.1 3.9 %collective-permute-start = (bf16[30,2048]{1,0:T(8,128)(2,1)S(1)}, bf16[30,2048]{1,0:T(8,128)(2,1)S(1)}, u32[]{:S(2)}, u32[]{:S(2)}) collective-permute-start(bf16[30,2048]{1,0:T(8,128)(2,1)S(1)} %slice.248), channel_id=1, source_target_pairs={{0,1},{1,2},{2,3},{3,4},{4,5},{5,6},{6,7},{7,8},{8,9},{9,10},{10,1... | collective-permute-start | bytes 368648 | tf_op jit(solution)/shard_map/ppermute | solution.py:436
  14.0 0.0 copy-done.1
  14.0 0.1 fusion.31
  14.1 0.1 fusion.30
  14.2 0.0 copy-done.2
  14.3 0.0 copy-done.5
  14.3 0.6 divide_bitcast_fusion.share
  14.9 4.1 %collective-permute-done = bf16[30,2048]{1,0:T(8,128)(2,1)S(1)} collective-permute-done((bf16[30,2048]{1,0:T(8,128)(2,1)S(1)}, bf16[30,2048]{1,0:T(8,128)(2,1)S(1)}, u32[]{:S(2)}, u32[]{:S(2)}) %collective-permute-start) | collective-permute-done | bytes 122912 | tf_op jit(solution)/shard_map/ppermute | solution.py:436
  19.0 0.0 copy-start.3
  19.0 0.0 copy-start.4
  19.0 14.3 %fusion.29 = (f32[384]{0:T(512)S(1)}, f32[384,2048]{1,0:T(8,128)S(1)}) fusion(bf16[384,2048]{1,0:T(8,128)(2,1)S(1)} %multiply_convert_fusion.1, bf16[30,2048]{1,0:T(8,128)(2,1)S(1)} %collective-permute-done, f32[2048]{0:T(1024)S(1)} %bitcast.51, f32[2048]{0:T(1024)S(1)} %bitcast.52, f32[2048]{0:T(1024)S(1)} %bitcast.54, f32[2048]{0:T(1024)S(1)} %bitcast.55, ...), kind=kLoop, calls=%fused_computation.73 | loop fusion | flops 143916672 | bytes 5096960 | tf_op jit(solution)/shard_map/reduce_sum | solution.py:444
  33.3 0.5 multiply_reduce_fusion
  33.8 0.0 copy-done.3
  33.8 0.0 copy-done.4
  33.8 2.4 multiply_convert_fusion
  36.2 0.0 all-gather.2.cloned.1.call-update
  36.2 270.4 %experts.1 = bf16[512,1024]{1,0:T(8,128)(2,1)} custom-call(bf16[512,4096]{1,0:T(8,128)(2,1)} %rows_hbm.1, f32[1,4096]{1,0:T(1,128)} %bitcast.72, s32[4,2,128]{2,1,0:T(2,128)} %bitcast.73, f32[4,2,128]{2,1,0:T(2,128)} %divide_bitcast_fusion.share, bf16[1,4096,256]{2,1,0:T(8,128)(2,1)} %gate_hbm.1, bf16[1,4096,256]{2,1,0:T(8,128)(2,1)} %up_hbm.1, ...), custom_call_target="tpu_custom_call" | custom-call | flops 149999992832 | bytes 16777216 | tf_op jit(solution)/shard_map/experts/pallas_call | solution.py:370
  306.7 0.0 copy-start
  306.7 0.0 all-gather.2.cloned.1.call-done
  306.7 11.2 %convolution_convert_fusion = bf16[1536,1024]{1,0:T(8,128)(2,1)} fusion(bf16[1536,2048]{1,0:T(8,128)(2,1)} %all-gather.2.cloned.1.call-done, bf16[2048,1024]{1,0:T(8,128)(2,1)} %param.19), kind=kOutput, calls=%fused_computation.29 | convolution fusion | flops 6444023808 | bytes 13631488 | tf_op jit(solution)/shard_map/dot_general | solution.py:458
  317.9 0.0 copy-done
  317.9 1.0 copy.17
  (4 shorter events, 0.1 us)
Async XLA Ops:
  7.2 6.9 %copy-start.1 = (f32[31,2048]{1,0:T(8,128)S(1)}, f32[31,2048]{1,0:T(8,128)}, u32[]{:S(2)}) copy-start(f32[31,2048]{1,0:T(8,128)} %param.16) | copy-start | bytes 761860
  7.2 7.1 %copy-start.2 = (f32[512,2]{0,1:T(2,128)S(1)}, f32[512,2]{0,1:T(2,128)}, u32[]{:S(2)}) copy-start(f32[512,2]{0,1:T(2,128)} %param.24) | copy-start | bytes 12292
  7.2 7.1 %copy-start.5 = (f32[512]{0:T(512)S(1)}, f32[512]{0:T(512)}, u32[]{:S(2)}) copy-start(f32[512]{0:T(512)} %param.23) | copy-start | bytes 6148
  7.2 299.5 %all-gather.2.cloned.1.call-start = ((), (), s32[]{:S(2)}) async-start(), calls=%async_computation | async-start | bytes 7864320 | tf_op jit(solution)/shard_map/all_gather | solution.py:454
  10.1 8.9 %collective-permute-start = (bf16[30,2048]{1,0:T(8,128)(2,1)S(1)}, bf16[30,2048]{1,0:T(8,128)(2,1)S(1)}, u32[]{:S(2)}, u32[]{:S(2)}) collective-permute-start(bf16[30,2048]{1,0:T(8,128)(2,1)S(1)} %slice.248), channel_id=1, source_target_pairs={{0,1},{1,2},{2,3},{3,4},{4,5},{5,6},{6,7},{7,8},{8,9},{9,10},{10,1... | collective-permute-start | bytes 368648 | tf_op jit(solution)/shard_map/ppermute | solution.py:436
  19.0 14.8 %copy-start.3 = (f32[2048]{0:T(1024)S(1)}, f32[2048]{0:T(1024)}, u32[]{:S(2)}) copy-start(f32[2048]{0:T(1024)} %param.18) | copy-start | bytes 24580
  19.0 14.8 %copy-start.4 = (f32[2048]{0:T(1024)S(1)}, f32[2048]{0:T(1024)}, u32[]{:S(2)}) copy-start(f32[2048]{0:T(1024)} %param.17) | copy-start | bytes 24580
  306.7 11.2 %copy-start = (bf16[512,1024]{1,0:T(8,128)(2,1)S(1)}, bf16[512,1024]{1,0:T(8,128)(2,1)}, u32[]{:S(2)}) copy-start(bf16[512,1024]{1,0:T(8,128)(2,1)} %experts.1) | copy-start | bytes 3145732
Sparse Core Ops, SparseCore 0:
  36.4 122.3 all-gather.1

commit v2 on v1

v2 whole, which is shorter than its diff:
```python
import jax
import jax.numpy as jnp
from jax import lax
from jax.experimental import pallas as pl
from jax.experimental.pallas import tpu as pltpu
from jax.sharding import PartitionSpec as P

EXPERTS = 32
TOP = 2
MOE_DEV = 128
CAP = 16
D = 4096
CONV = 2048
KERNEL = 31
ROWS = 384
HALO = 32
BLOCK = 128
HID_PART = 256
OUT_PART = 1024
EP_TP = ("ep", "tp")
MESH = pl.DeviceIdType.MESH
BF16 = jnp.bfloat16
F32 = jnp.float32

epsilon = 1e-06

BUFFER = {(0, 0): 0, (0, 1): 1, (1, 0): 2, (3, 1): 3, (1, 1): 4, (3, 0): 5, (2, 0): 0, (2, 1): 1}
RESULT = {0: 0, 1: 1, 3: 0, 2: 1}
PAIRS = [((0, 0), (0, 1)), ((1, 0), (3, 1)), ((3, 0), (1, 1)), ((2, 0), (2, 1))]
Y_ORDER = [(0, 1), (1, 0), (3, 0), (1, 1), (3, 1), (2, 0), (2, 1)]


def kernel(
    value_hbm,
    gate_rows_hbm,
    taps,
    conv_gain,
    conv_bias,
    projection_hbm,
    rows_hbm,
    gain,
    route,
    share,
    gate_hbm,
    up_hbm,
    down_hbm,
    conv_out,
    out_hbm,
    tokens,
    slots,
    arrived,
    w_gate,
    w_up,
    w_down,
    hidden,
    result,
    back,
    partial,
    landed,
    out,
    meta,
    acc_gate,
    acc_up,
    gated,
    mixed,
    w_conv,
    load_sem,
    z_send,
    z_recv,
    m_send,
    m_recv,
    y_send,
    y_recv,
    x_send,
    x_recv,
    h_send,
    h_recv,
    b_send,
    b_recv,
    p_send,
    p_recv,
    halo_sem,
    c_send,
    c_recv,
    store_sem,
    out_sem,
    free_sem,
):
    ep = lax.axis_index("ep")
    x = lax.axis_index("tp")
    z, y, c = ep // 8, (ep // 2) % 4, ep % 2

    def at(dz, dy, dc, dx):
        there = (((z + dz) % 4) * 4 + (y + dy) % 4) * 2 + (c + dc) % 2
        return (there, (x + dx) % 4)

    def remote(src, dst, send, recv, device):
        return pltpu.make_async_remote_copy(
            src_ref=src, dst_ref=dst, send_sem=send, recv_sem=recv, device_id=device, device_id_type=MESH
        )

    quarter = (x, (x + 1) % 4)
    number = ep * 4 + x
    after, ahead = (number + 1) % 128, (number + 127) % 128

    raw = [
        pltpu.make_async_copy(
            rows_hbm.at[pl.ds(pl.multiple_of(quarter[i] * MOE_DEV, MOE_DEV), MOE_DEV)],
            slots.at[2 + i],
            load_sem.at[i],
        )
        for i in range(2)
    ]
    value_load = pltpu.make_async_copy(value_hbm, gated.at[pl.ds(HALO, ROWS)], load_sem.at[2])
    gate_loads = [
        pltpu.make_async_copy(
            gate_rows_hbm.at[pl.ds(b * BLOCK, BLOCK)],
            slots.at[4 + b // 2, :, pl.ds((b % 2) * CONV, CONV)],
            load_sem.at[3 + b],
        )
        for b in range(3)
    ]
    weights = [
        pltpu.make_async_copy(gate_hbm.at[0], w_gate, load_sem.at[6]),
        pltpu.make_async_copy(up_hbm.at[0], w_up, load_sem.at[7]),
        pltpu.make_async_copy(down_hbm.at[0], w_down, load_sem.at[8]),
        pltpu.make_async_copy(projection_hbm, w_conv, load_sem.at[9]),
    ]
    for load in raw + [value_load] + gate_loads + weights:
        load.start()

    barrier = pltpu.get_barrier_semaphore()
    partners = [at(dz, 0, 0, 0) for dz in (1, 2, 3)]
    partners += [at(0, dy, dc, 0) for dy in range(4) for dc in range(2) if dy or dc]
    partners += [at(0, 0, 0, dx) for dx in (1, 2, 3)]
    partners += [(after // 4, after % 4), (ahead // 4, ahead % 4)]
    for device in partners:
        pl.semaphore_signal(barrier, inc=1, device_id=device, device_id_type=MESH)

    lane = lax.broadcasted_iota(jnp.int32, (128, 128), 1)
    sub = lax.broadcasted_iota(jnp.int32, (128, 128), 0)
    earlier = jnp.where(sub < lane, 1.0, 0.0).astype(BF16)
    expert_row = lax.broadcasted_iota(jnp.int32, (EXPERTS, 128), 0)
    for q in range(4):
        first, second = route[q, 0:1, :], route[q, 1:2, :]
        hot0 = jnp.where(expert_row == first, 1.0, 0.0)
        hot1 = jnp.where(expert_row == second, 1.0, 0.0)
        before = jnp.dot((hot0 + hot1).astype(BF16), earlier, preferred_element_type=F32)
        pos0 = jnp.sum(before * hot0, axis=0, keepdims=True)
        pos1 = jnp.sum(before * hot1, axis=0, keepdims=True)
        meta[0, q, 0:1, :] = first.astype(F32) * CAP + pos0
        meta[0, q, 1:2, :] = second.astype(F32) * CAP + pos1
        meta[0, q, 2:4, :] = share[q]
        meta[0, q, 4:8, :] = jnp.zeros((4, 128), F32)

    for i in range(2):
        raw[i].wait()

        @pl.loop(0, 8)
        def _(t):
            r = pl.ds(pl.multiple_of(t * 16, 16), 16)
            wide = slots[2 + i, r, :].astype(F32)
            inverse = lax.rsqrt(jnp.mean(wide * wide, axis=-1, keepdims=True) + epsilon)
            tokens[0, i, r, :] = (wide * inverse * gain[...]).astype(BF16)

    pl.semaphore_wait(barrier, len(partners))

    meta_copies = {
        dz: remote(meta.at[0], meta.at[dz], m_send.at[dz], m_recv.at[dz], at(dz, 0, 0, 0)) for dz in (1, 2, 3)
    }
    for dz in (1, 3, 2):
        meta_copies[dz].start()

    def z_copy(dz, i):
        if dz == 2:
            source, step = (1, 1) if i == 0 else (3, 3)
        else:
            source, step = 0, dz
        return remote(tokens.at[source, i], tokens.at[dz, i], z_send.at[dz, i], z_recv.at[dz, i], at(step, 0, 0, 0))

    for dz, i in ((1, 0), (3, 1), (1, 1), (3, 0)):
        z_copy(dz, i).start()

    plane = (z * 128).astype(F32)
    slot_row = lax.broadcasted_iota(jnp.int32, (128, 128), 0).astype(F32)

    def y_copy(dz, i, dy, dc):
        there = ((y + dy) % 4) * 2 + (c + dc) % 2
        k = dy * 2 + dc
        return remote(
            slots.at[BUFFER[dz, i], pl.ds(pl.multiple_of(there * CAP, CAP), CAP)],
            arrived.at[dz, k, quarter[i]],
            y_send.at[dz, i, k],
            y_recv.at[dz, i, k],
            at(0, dy, dc, 0),
        )

    def build(dz, i):
        q = quarter[i]
        if dz == 2:
            for dy, dc in Y_ORDER:
                y_copy(0, i, dy, dc).wait_send()
        hot = jnp.where(slot_row == meta[dz, q, 0:1, :] - plane, 1.0, 0.0)
        hot = hot + jnp.where(slot_row == meta[dz, q, 1:2, :] - plane, 1.0, 0.0)
        hot = hot.astype(BF16)

        @pl.loop(0, D // 512)
        def _(t):
            cols = pl.ds(pl.multiple_of(t * 512, 512), 512)
            slots[BUFFER[dz, i], :, cols] = jnp.dot(
                hot, tokens[dz, i, :, cols], preferred_element_type=F32
            ).astype(BF16)


    def send_slots(pair):
        for dy, dc in Y_ORDER:
            for dz, i in pair:
                y_copy(dz, i, dy, dc).start()
        own = pl.ds(pl.multiple_of((y * 2 + c) * CAP, CAP), CAP)
        for dz, i in pair:
            arrived[dz, 0, quarter[i]] = slots[BUFFER[dz, i], own, :]

    def take_z(dz, i):
        z_copy(dz, i).wait_recv()

    def x_copy(dz, i, k):
        q = quarter[i]
        return remote(
            arrived.at[dz, k, q],
            arrived.at[dz, k, q],
            x_send.at[dz, i, k],
            x_recv.at[dz, i, k],
            at(0, 0, 0, 1 if i == 0 else 3),
        )

    def pass_on(pair, between):
        for dz, i in pair:
            x_copy(dz, i, 0).start()
        for step, (dy, dc) in enumerate(Y_ORDER):
            for work in between.get(step, ()):
                work()
            for dz, i in pair:
                y_copy(dz, i, dy, dc).wait_recv()
                x_copy(dz, i, dy * 2 + dc).start()

    def x_landing(dz, i, k):
        q = (x + 3) % 4 if i == 0 else (x + 2) % 4
        return remote(
            arrived.at[dz, k, q],
            arrived.at[dz, k, q],
            x_send.at[dz, i, k],
            x_recv.at[dz, i, k],
            at(0, 0, 0, 3 if i == 0 else 1),
        )

    def h_copy(g, way, source):
        half = pl.ds(0, 512) if way < 2 else pl.ds((way - 2) * 256, 256)
        piece = hidden.at[g, source, half]
        return remote(
            piece, piece, h_send.at[g, way], h_recv.at[g, way], at(0, 0, 0, 1 if way % 2 == 0 else 3)
        )

    KB = 512

    def first_product(g):
        for i in range(2):
            for k in range(8):
                x_landing(g, i, k).wait_recv()
        acc_gate[...] = jnp.zeros_like(acc_gate)
        acc_up[...] = jnp.zeros_like(acc_up)

        @pl.loop(0, D // KB)
        def _(t):
            cols = pl.ds(pl.multiple_of(t * KB, KB), KB)
            piece = arrived[g, :, :, :, cols].reshape(512, KB)
            acc_gate[...] += jnp.dot(piece, w_gate[cols, :], preferred_element_type=F32)
            acc_up[...] += jnp.dot(piece, w_up[cols, :], preferred_element_type=F32)

        @pl.loop(0, 8)
        def _(t):
            r = pl.ds(pl.multiple_of(t * 64, 64), 64)
            gate = acc_gate[r, :]
            hidden[g, x, r, :] = (gate / (1.0 + jnp.exp(-gate)) * acc_up[r, :]).astype(BF16)

        for way in (0, 1):
            h_copy(g, way, x).start()

    def pass_hidden(g):
        h_copy(g, 0, (x + 3) % 4).wait_recv()
        h_copy(g, 2, (x + 3) % 4).start()
        h_copy(g, 1, (x + 1) % 4).wait_recv()
        h_copy(g, 3, (x + 1) % 4).start()

    def b_copy(g, dy, dc):
        k = dy * 2 + dc
        return remote(
            result.at[RESULT[g], k],
            back.at[g, :, y * 2 + c],
            b_send.at[g, k],
            b_recv.at[g, k],
            at(0, (4 - dy) % 4, dc, 0),
        )

    def b_landing(g, dy, dc):
        k = dy * 2 + dc
        source = ((y + dy) % 4) * 2 + (c + dc) % 2
        return remote(
            result.at[RESULT[g], k],
            back.at[g, :, source],
            b_send.at[g, k],
            b_recv.at[g, k],
            at(0, (4 - dy) % 4, dc, 0),
        )

    def second_product(g):
        for way in (2, 3):
            h_copy(g, way, (x + 2) % 4).wait_recv()
        if g >= 2:
            for dy, dc in Y_ORDER:
                b_copy(0 if g == 3 else 1, dy, dc).wait_send()

        @pl.loop(0, OUT_PART // 256)
        def _(t):
            cols = pl.ds(pl.multiple_of(t * 256, 256), 256)
            total = jnp.dot(hidden[g, 0], w_down[0:256, cols], preferred_element_type=F32)
            for s in range(1, 4):
                total += jnp.dot(hidden[g, s], w_down[s * 256 : (s + 1) * 256, cols], preferred_element_type=F32)
            result[RESULT[g], :, :, :, cols] = total.astype(BF16).reshape(8, 4, CAP, 256)

        for dy, dc in Y_ORDER:
            b_copy(g, dy, dc).start()
        back[g, :, y * 2 + c] = result[RESULT[g], 0]

    def p_copy(g):
        return remote(partial.at[g - 1], landed.at[g - 1], p_send.at[g], p_recv.at[g], at(4 - g, 0, 0, 0))

    def combine(g):
        for dy, dc in Y_ORDER:
            b_landing(g, dy, dc).wait_recv()

        @pl.loop(0, 4)
        def _(q):
            weight = jnp.where(slot_row == meta[g, q, 0:1, :] - plane, meta[g, q, 2:3, :], 0.0)
            weight = weight + jnp.where(slot_row == meta[g, q, 1:2, :] - plane, meta[g, q, 3:4, :], 0.0)
            high = weight.astype(BF16)
            low = (weight - high.astype(F32)).astype(BF16)
            rows = back[g, q].reshape(128, OUT_PART)
            dims = (((0,), (0,)), ((), ()))
            total = lax.dot_general(high, rows, dims, preferred_element_type=F32)
            total += lax.dot_general(low, rows, dims, preferred_element_type=F32)
            r = pl.ds(pl.multiple_of(q * 128, 128), 128)
            if g:
                partial[g - 1, r, :] = total.astype(BF16)
            else:
                out[r, :] = total.astype(BF16)

        if g:
            p_copy(g).start()

    def out_store(part):
        r = pl.ds(part * 128, 128)
        return pltpu.make_async_copy(out.at[r], out_hbm.at[r], out_sem.at[part])

    def final_sum():
        for g in (1, 3, 2):
            p_copy(g).wait_recv()
        for part in range(4):

            @pl.loop(0, 4)
            def _(t):
                r = pl.ds(pl.multiple_of(part * 128 + t * 32, 32), 32)
                total = out[r, :].astype(F32) + landed[0, r, :].astype(F32)
                total = total + landed[1, r, :].astype(F32) + landed[2, r, :].astype(F32)
                out[r, :] = total.astype(BF16)

            out_store(part).start()

    halo = remote(
        gated.at[pl.ds(ROWS, HALO)], gated.at[pl.ds(0, HALO)], halo_sem.at[0], halo_sem.at[1], (after // 4, after % 4)
    )

    def conv_gate():
        value_load.wait()
        for load in gate_loads:
            load.wait()
        for b in range(3):

            @pl.loop(0, BLOCK // 16)
            def _(t):
                r = pl.ds(pl.multiple_of(t * 16, 16), 16)
                to = pl.ds(pl.multiple_of(HALO + b * BLOCK + t * 16, 16), 16)
                gate = slots[4 + b // 2, r, (b % 2) * CONV : (b % 2 + 1) * CONV].astype(F32)
                gated[to, :] = (gated[to, :].astype(F32) / (1.0 + jnp.exp(-gate))).astype(BF16)

        halo.start()

    tile_row = lax.broadcasted_iota(jnp.int32, (8, 128), 0)

    def take_halo():
        halo.wait_recv()

        @pl.when(number == 0)
        def _():
            gated[0:HALO, :] = jnp.zeros((HALO, CONV), BF16)

    def conv_columns(b, half):
        @pl.loop(half * (CONV // 256), (half + 1) * (CONV // 256))
        def _(t):
            cols = pl.ds(pl.multiple_of(t * 128, 128), 128)
            tap = [jnp.broadcast_to(taps[j : j + 1, cols], (8, 128)) for j in range(KERNEL)]
            tiles = []
            last = None
            for n in range((HALO + BLOCK) // 16):
                pair = gated[b * BLOCK + n * 16 : b * BLOCK + (n + 1) * 16, cols].astype(F32)
                for half in (pair[0:8], pair[8:16]):
                    tiles.append(half)
                    count = len(tiles)
                    if count < 4:
                        continue
                    sums = []
                    for j in range(8):
                        total = tap[j] * tiles[count - 1]
                        for a in range(1, 4):
                            if 8 * a + j < KERNEL:
                                total = total + tap[8 * a + j] * tiles[count - 1 - a]
                        sums.append(total)
                    if count > 4:
                        total = sums[0]
                        for j in range(1, 8):
                            total = total + pltpu.roll(jnp.where(tile_row >= 8 - j, last[j], sums[j]), j, 0)
                        row = (count - 5) * 8
                        mixed[row : row + 8, cols] = total
                    last = sums

    def conv_norm(b):
        @pl.loop(0, BLOCK // 16)
        def _(t):
            r = pl.ds(pl.multiple_of(t * 16, 16), 16)
            wide = mixed[r, :]
            center = wide - jnp.mean(wide, axis=-1, keepdims=True)
            spread = jnp.mean(center * center, axis=-1, keepdims=True)
            unit = center * lax.rsqrt(spread + epsilon) * conv_gain[...] + conv_bias[...]
            to = pl.ds(pl.multiple_of(b * BLOCK + t * 16, 16), 16)
            gated[to, :] = (unit / (1.0 + jnp.exp(-unit))).astype(BF16)

    def held(source, b, start=0, rows=BLOCK):
        return tokens.at[source, b // 2, pl.ds(start, rows), pl.ds((b % 2) * CONV, CONV)]

    def c_copy(way, b):
        return remote(
            gated.at[pl.ds(b * BLOCK, BLOCK)],
            held(x, b),
            c_send.at[way, b],
            c_recv.at[way, b],
            at(0, 0, 0, 1 if way == 0 else 3),
        )

    def c_landing(way, b):
        place = held((x + 3) % 4 if way == 0 else (x + 1) % 4, b)
        return remote(place, place, c_send.at[way, b], c_recv.at[way, b], at(0, 0, 0, 1 if way == 0 else 3))

    def c_pass(way, part, source):
        place = held(source, way - 2) if part == 0 else held(source, 2, (way - 2) * 64, 64)
        return remote(place, place, c_send.at[way, part], c_recv.at[way, part], at(0, 0, 0, 1 if way == 2 else 3))

    def free_tokens():
        for dz in (1, 2, 3):
            for i in range(2):
                z_copy(dz, i).wait_send()
        for dx in (1, 2, 3):
            pl.semaphore_signal(free_sem, inc=1, device_id=at(0, 0, 0, dx), device_id_type=MESH)

    def conv_send():
        pl.semaphore_wait(free_sem, 3)
        for turn in range(3):
            for way in range(2):
                c_copy(way, ((0, 2, 1), (1, 2, 0))[way][turn]).start()

    def conv_pass():
        c_landing(0, 0).wait_recv()
        c_pass(2, 0, (x + 3) % 4).start()
        c_landing(1, 1).wait_recv()
        c_pass(3, 0, (x + 1) % 4).start()
        c_landing(0, 2).wait_recv()
        c_pass(2, 1, (x + 3) % 4).start()
        c_landing(1, 2).wait_recv()
        c_pass(3, 1, (x + 1) % 4).start()

    def staged(dx, b):
        n = 3 * dx + b
        return n // 4, pl.ds((n % 4) * OUT_PART, OUT_PART)

    def conv_store(dx, b):
        source = (x + dx) % 4
        buffer, cols = staged(dx, b)
        return pltpu.make_async_copy(
            slots.at[buffer, :, cols],
            conv_out.at[pl.ds(pl.multiple_of(source * ROWS + b * BLOCK, BLOCK), BLOCK)],
            store_sem.at[dx, b],
        )

    def conv_product(dx, blocks=(0, 1, 2)):
        source = (x + dx) % 4
        if dx == 3:
            c_landing(0, 1).wait_recv()
        if dx == 1:
            c_landing(1, 0).wait_recv()
        for b in blocks:
            if dx == 2:
                for way, part in (((2, 0),), ((3, 0),), ((2, 1), (3, 1)))[b]:
                    c_pass(way, part, source).wait_recv()
            buffer, _ = staged(dx, b)
            base = ((3 * dx + b) % 4) * OUT_PART

            @pl.loop(0, OUT_PART // 256)
            def _(t):
                cols = pl.ds(pl.multiple_of(t * 256, 256), 256)
                to = pl.ds(pl.multiple_of(base + t * 256, 256), 256)
                if dx:
                    block = tokens[source, b // 2, :, (b % 2) * CONV : (b % 2 + 1) * CONV]
                else:
                    block = gated[b * BLOCK : (b + 1) * BLOCK, :]
                slots[buffer, :, to] = jnp.dot(block, w_conv[:, cols], preferred_element_type=F32).astype(BF16)

            conv_store(dx, b).start()

    def y_left():
        for dz in range(1, 4):
            for i in range(2):
                for dy, dc in Y_ORDER:
                    y_copy(dz, i, dy, dc).wait_send()

    def drain():
        for dz in (1, 2, 3):
            meta_copies[dz].wait_send()
        halo.wait_send()
        for g in range(4):
            for way in range(4):
                h_copy(g, way, (x, x, (x + 3) % 4, (x + 1) % 4)[way]).wait_send()
            if g >= 2:
                for dy, dc in Y_ORDER:
                    b_copy(g, dy, dc).wait_send()
            for i in range(2):
                for k in range(8):
                    x_copy(g, i, k).wait_send()
        for way in range(2):
            for b in range(3):
                c_copy(way, b).wait_send()
        for dx in (0, 1, 3):
            for b in range(3):
                conv_store(dx, b).wait()

    def finish():
        for dz in (1, 2, 3):
            p_copy(dz).wait_send()
        for way in range(2):
            for part in range(2):
                c_pass(way + 2, part, (x + 3) % 4 if way == 0 else (x + 1) % 4).wait_send()
        for part in range(4):
            out_store(part).wait()
        for b in range(3):
            conv_store(2, b).wait()

    def build_pair(number):
        for dz, i in PAIRS[number]:
            if number:
                take_z(dz, i)
            if number == 1:
                z_copy(2, i).start()
        if number == 1:
            meta_copies[1].wait_recv()
            meta_copies[3].wait_recv()
        if number == 3:
            meta_copies[2].wait_recv()
        for dz, i in PAIRS[number]:
            build(dz, i)
        send_slots(PAIRS[number])

    def pass_pair(number, between):
        pass_on(PAIRS[number], between)

    def wait_weights():
        for load in weights:
            load.wait()

    build_pair(0)
    conv_gate()
    conv_work = {0: [], 1: [take_halo]}
    for b in range(3):
        conv_work.setdefault(2 * b + 1, []).append(lambda b=b: conv_columns(b, 0))
        conv_work.setdefault(2 * b + 2, []).append(lambda b=b: conv_columns(b, 1))
        conv_work[2 * b + 2].append(lambda b=b: conv_norm(b))
    pass_pair(0, conv_work)
    build_pair(1)
    pass_pair(1, {3: [wait_weights, lambda: first_product(0)]})
    build_pair(2)
    pass_pair(2, {5: [lambda: build_pair(3)]})
    pass_pair(
        3,
        {
            0: [lambda: pass_hidden(0)],
            1: [lambda: first_product(1)],
            2: [lambda: first_product(3)],
            3: [lambda: second_product(0)],
            5: [lambda: pass_hidden(1)],
            6: [lambda: pass_hidden(3)],
        },
    )
    free_tokens()
    second_product(1)
    second_product(3)
    combine(0)
    first_product(2)
    combine(1)
    pass_hidden(2)
    conv_send()
    combine(3)
    second_product(2)
    y_left()
    conv_product(0)
    combine(2)
    conv_pass()
    conv_product(3)
    conv_product(1)
    drain()
    final_sum()
    conv_product(2, (0, 1))
    conv_product(2, (2,))
    finish()


def both_branches(*operands):
    vmem, hbm = pl.BlockSpec(memory_space=pltpu.VMEM), pl.BlockSpec(memory_space=pl.ANY)
    dma = pltpu.SemaphoreType.DMA
    return pl.pallas_call(
        kernel,
        name="experts",
        out_shape=(
            jax.ShapeDtypeStruct((4 * ROWS, OUT_PART), BF16),
            jax.ShapeDtypeStruct((512, OUT_PART), BF16),
        ),
        in_specs=[hbm, hbm, vmem, vmem, vmem, hbm, hbm, vmem, vmem, vmem, hbm, hbm, hbm],
        out_specs=(hbm, hbm),
        scratch_shapes=[
            pltpu.VMEM((4, 2, 128, D), BF16),
            pltpu.VMEM((6, 128, D), BF16),
            pltpu.VMEM((4, 8, 4, CAP, D), BF16),
            pltpu.VMEM((D, HID_PART), BF16),
            pltpu.VMEM((D, HID_PART), BF16),
            pltpu.VMEM((1024, OUT_PART), BF16),
            pltpu.VMEM((4, 4, 512, HID_PART), BF16),
            pltpu.VMEM((2, 8, 4, CAP, OUT_PART), BF16),
            pltpu.VMEM((4, 4, 8, CAP, OUT_PART), BF16),
            pltpu.VMEM((3, 512, OUT_PART), BF16),
            pltpu.VMEM((3, 512, OUT_PART), BF16),
            pltpu.VMEM((512, OUT_PART), BF16),
            pltpu.VMEM((4, 4, 8, 128), F32),
            pltpu.VMEM((512, HID_PART), F32),
            pltpu.VMEM((512, HID_PART), F32),
            pltpu.VMEM((HALO + ROWS, CONV), BF16),
            pltpu.VMEM((BLOCK, CONV), F32),
            pltpu.VMEM((CONV, OUT_PART), BF16),
            dma((10,)),
            dma((4, 2)),
            dma((4, 2)),
            dma((4,)),
            dma((4,)),
            dma((4, 2, 8)),
            dma((4, 2, 8)),
            dma((4, 2, 8)),
            dma((4, 2, 8)),
            dma((4, 4)),
            dma((4, 4)),
            dma((4, 8)),
            dma((4, 8)),
            dma((4,)),
            dma((4,)),
            dma((2,)),
            dma((4, 3)),
            dma((4, 3)),
            dma((4, 3)),
            dma((4,)),
            pltpu.SemaphoreType.REGULAR,
        ],
        compiler_params=pltpu.CompilerParams(
            collective_id=0, has_side_effects=True, vmem_limit_bytes=67_043_328
        ),
        cost_estimate=pl.CostEstimate(flops=150_000_000_000, bytes_accessed=16 << 20, transcendentals=0),
    )(*operands)


def on_device(
    conv_value,
    conv_gate,
    conv_taps,
    conv_gain,
    conv_bias,
    conv_projection,
    expert_input,
    expert_gain,
    route_experts,
    group_gate,
    expert_gate,
    gate_weight,
    up_weight,
    down_weight,
):
    route_share = group_gate[:, None] * expert_gate / jnp.sum(expert_gate, axis=1, keepdims=True)
    route = route_experts.reshape(4, MOE_DEV, TOP).transpose(0, 2, 1)
    share = route_share.reshape(4, MOE_DEV, TOP).transpose(0, 2, 1)
    return both_branches(
        conv_value,
        conv_gate,
        conv_taps,
        conv_gain[None],
        conv_bias[None],
        conv_projection,
        expert_input,
        expert_gain[None],
        route,
        share,
        gate_weight,
        up_weight,
        down_weight,
    )


def solution(mesh):
    in_specs = (
        P(EP_TP, None),
        P(EP_TP, None),
        P(),
        P(),
        P(),
        P(None, "tp"),
        P("ep", None),
        P(),
        P("ep", None),
        P("ep"),
        P("ep", None),
        P("ep", None, "tp"),
        P("ep", None, "tp"),
        P("ep", None, "tp"),
    )
    out_specs = (P("ep", "tp"), P("ep", "tp"))
    return jax.shard_map(
        on_device, mesh=mesh, in_specs=in_specs, out_specs=out_specs, check_vma=False
    )
```

time: 326 us -> 225 us (0.69)
  Pallas kernels: 270 us -> 216 us
  other arithmetic: 20.6 us -> 2.01 us
  between operations: 14.2 us -> 0.65 us
  matrix products: 11.2 us -> 0 us
  waiting for transfers between devices: 4.15 us -> 0 us
  starting transfers between devices: 3.97 us -> 0 us
  local copies, waits for them, and re-layouts: 1.21 us -> 4.92 us
    pallas_call x1, Pallas kernels: 270 us -> 216 us  [both_branches(): pl.pallas_call(kernel, name='experts', out_shape=(jax.ShapeDtypeStruct((4...]
    reduce_sum x2 -> x0, other arithmetic: 14.8 us -> none  [the longest x1 14.3 us: on_device(): center = mixed_conv - jnp.mean(mixed_conv, axis=-1, keepdims=True)]
    dot_general x1 -> x0, matrix products: 11.2 us -> none  [on_device(): jnp.dot(gathered, conv_projection, preferred_element_type=jnp.float32)]
    convert_element_type x2 -> x0, other arithmetic: 5.19 us -> none  [the longest x1 2.81 us: on_device(): gated_rows = (conv_value.astype(jnp.float32) * jax.nn.sigmoid(conv_gate.a...]
    ppermute x1 -> x0, waiting for transfers between devices: 4.11 us -> none  [on_device(): lax.ppermute(gated_rows[length - reach_back:], EP_TP, [(s, s + 1) for s i...]
    ppermute x1 -> x0, starting transfers between devices: 3.94 us -> none  [on_device(): lax.ppermute(gated_rows[length - reach_back:], EP_TP, [(s, s + 1) for s i...]
    unnamed x13 -> x4, local copies, waits for them, and re-layouts: 0.99 us -> 4.92 us
  transfers between devices with their start and end apart: 2 -> 0, of which waited for: 1 -> 0; matrix products, arithmetic and copies ran while one was open for 0% -> 0% of each run, Pallas kernels for 83% -> 0%
where the time goes in v2:
time: 225 us; the launch traced here: 223 us
  Pallas kernels  216 us (96%)
  local copies, waits for them, and re-layouts  4.92 us (2%)
    pallas_call x1, Pallas kernels, both_branches(): pl.pallas_call(kernel, name='experts', out_shape=(jax.ShapeDtypeStruct((4...  216 us
    unnamed x4, local copies, waits for them, and re-layouts  4.92 us

profile of v2, /device:TPU:1, one launch (start us, length us, event | category | flops | bytes accessed | tf_op | source)
XLA Modules:
  0.0 223.2 jit_solution(4157862207265123071)
XLA Ops:
  0.6 0.7 reduce_sum.9
  1.3 1.3 divide_bitcast_fusion.share
  2.6 215.6 %experts.1 = (bf16[1536,1024]{1,0:T(8,128)(2,1)}, bf16[512,1024]{1,0:T(8,128)(2,1)}) custom-call(bf16[384,2048]{1,0:T(8,128)(2,1)} %value_hbm.1, bf16[384,2048]{1,0:T(8,128)(2,1)} %gate_rows_hbm.1, f32[31,2048]{1,0:T(8,128)} %taps.1, f32[1,2048]{1,0:T(1,128)} %bitcast.11, f32[1,2048]{1,0:T(1,128)} %bitcast.12, bf16[2048,1024]{1,0:T(8,128)(2,1)} %projection_hbm.1, ...), custom_call_target="tpu_custom_call" | custom-call | flops 149999992832 | bytes 16777216 | tf_op jit(solution)/shard_map/experts/pallas_call | solution.py:635
  218.3 0.0 copy-start
  218.3 3.9 %copy.18 = bf16[1536,1024]{1,0:T(8,128)(2,1)} copy(bf16[1536,1024]{1,0:T(8,128)(2,1)} %get-tuple-element.4) | data formatting | bytes 6291456
  222.2 0.0 copy-done
  222.2 1.0 copy.19
Async XLA Ops:
  218.3 4.0 %copy-start = (bf16[512,1024]{1,0:T(8,128)(2,1)S(1)}, bf16[512,1024]{1,0:T(8,128)(2,1)}, u32[]{:S(2)}) copy-start(bf16[512,1024]{1,0:T(8,128)(2,1)} %get-tuple-element.5) | copy-start | bytes 3145732

commit v3 on v2

--- a/solution.py
+++ b/solution.py
@@ -40,7 +40,8 @@
     rows_hbm,
     gain,
     route,
-    share,
+    group_gate,
+    expert_gate,
     gate_hbm,
     up_hbm,
     down_hbm,
@@ -142,7 +143,9 @@
     earlier = jnp.where(sub < lane, 1.0, 0.0).astype(BF16)
     expert_row = lax.broadcasted_iota(jnp.int32, (EXPERTS, 128), 0)
     for q in range(4):
-        first, second = route[q, 0:1, :], route[q, 1:2, :]
+        lanes = slice(q * MOE_DEV, (q + 1) * MOE_DEV)
+        first, second = route[0:1, lanes], route[1:2, lanes]
+        gates = expert_gate[:, lanes]
         hot0 = jnp.where(expert_row == first, 1.0, 0.0)
         hot1 = jnp.where(expert_row == second, 1.0, 0.0)
         before = jnp.dot((hot0 + hot1).astype(BF16), earlier, preferred_element_type=F32)
@@ -150,7 +153,7 @@
         pos1 = jnp.sum(before * hot1, axis=0, keepdims=True)
         meta[0, q, 0:1, :] = first.astype(F32) * CAP + pos0
         meta[0, q, 1:2, :] = second.astype(F32) * CAP + pos1
-        meta[0, q, 2:4, :] = share[q]
+        meta[0, q, 2:4, :] = group_gate[:, lanes] * gates / jnp.sum(gates, axis=0, keepdims=True)
         meta[0, q, 4:8, :] = jnp.zeros((4, 128), F32)
 
     for i in range(2):
@@ -190,16 +193,19 @@
         return remote(
             slots.at[BUFFER[dz, i], pl.ds(pl.multiple_of(there * CAP, CAP), CAP)],
             arrived.at[dz, k, quarter[i]],
-            y_send.at[dz, i, k],
+            y_send.at[dz, i],
             y_recv.at[dz, i, k],
             at(0, dy, dc, 0),
         )
+
+    def y_left(dz, i):
+        sent = slots.at[BUFFER[dz, i], pl.ds(0, 7 * CAP)]
+        remote(sent, sent, y_send.at[dz, i], y_recv.at[dz, i, 0], at(0, 1, 0, 0)).wait_send()
 
     def build(dz, i):
         q = quarter[i]
         if dz == 2:
-            for dy, dc in Y_ORDER:
-                y_copy(0, i, dy, dc).wait_send()
+            y_left(0, i)
         hot = jnp.where(slot_row == meta[dz, q, 0:1, :] - plane, 1.0, 0.0)
         hot = hot + jnp.where(slot_row == meta[dz, q, 1:2, :] - plane, 1.0, 0.0)
         hot = hot.astype(BF16)
@@ -228,8 +234,8 @@
         return remote(
             arrived.at[dz, k, q],
             arrived.at[dz, k, q],
-            x_send.at[dz, i, k],
-            x_recv.at[dz, i, k],
+            x_send.at[dz, i],
+            x_recv.at[dz, i],
             at(0, 0, 0, 1 if i == 0 else 3),
         )
 
@@ -243,29 +249,28 @@
                 y_copy(dz, i, dy, dc).wait_recv()
                 x_copy(dz, i, dy * 2 + dc).start()
 
-    def x_landing(dz, i, k):
-        q = (x + 3) % 4 if i == 0 else (x + 2) % 4
-        return remote(
-            arrived.at[dz, k, q],
-            arrived.at[dz, k, q],
-            x_send.at[dz, i, k],
-            x_recv.at[dz, i, k],
-            at(0, 0, 0, 3 if i == 0 else 1),
-        )
+    def x_all(dz, i, q):
+        place = arrived.at[dz, :, q]
+        return remote(place, place, x_send.at[dz, i], x_recv.at[dz, i], at(0, 0, 0, 3 if i == 0 else 1))
+
+    def x_landed(dz, i):
+        x_all(dz, i, (x + 3) % 4 if i == 0 else (x + 2) % 4).wait_recv()
+
+    def x_left(dz, i):
+        x_all(dz, i, quarter[i]).wait_send()
 
     def h_copy(g, way, source):
         half = pl.ds(0, 512) if way < 2 else pl.ds((way - 2) * 256, 256)
         piece = hidden.at[g, source, half]
         return remote(
-            piece, piece, h_send.at[g, way], h_recv.at[g, way], at(0, 0, 0, 1 if way % 2 == 0 else 3)
+            piece, piece, h_send.at[g], h_recv.at[g, way], at(0, 0, 0, 1 if way % 2 == 0 else 3)
         )
 
     KB = 512
 
     def first_product(g):
         for i in range(2):
-            for k in range(8):
-                x_landing(g, i, k).wait_recv()
+            x_landed(g, i)
         acc_gate[...] = jnp.zeros_like(acc_gate)
         acc_up[...] = jnp.zeros_like(acc_up)
 
@@ -291,33 +296,29 @@
         h_copy(g, 1, (x + 1) % 4).wait_recv()
         h_copy(g, 3, (x + 1) % 4).start()
 
-    def b_copy(g, dy, dc):
-        k = dy * 2 + dc
+    def b_copy(g, dy, dc, half):
+        pick = pl.ds(half * 2, 2)
         return remote(
-            result.at[RESULT[g], k],
-            back.at[g, :, y * 2 + c],
-            b_send.at[g, k],
-            b_recv.at[g, k],
+            result.at[RESULT[g], dy * 2 + dc, pick],
+            back.at[g, pick, y * 2 + c],
+            b_send.at[g],
+            b_recv.at[g, half],
             at(0, (4 - dy) % 4, dc, 0),
         )
 
-    def b_landing(g, dy, dc):
-        k = dy * 2 + dc
-        source = ((y + dy) % 4) * 2 + (c + dc) % 2
-        return remote(
-            result.at[RESULT[g], k],
-            back.at[g, :, source],
-            b_send.at[g, k],
-            b_recv.at[g, k],
-            at(0, (4 - dy) % 4, dc, 0),
-        )
+    def b_left(g):
+        sent = result.at[RESULT[g], pl.ds(1, 7)]
+        remote(sent, sent, b_send.at[g], b_recv.at[g, 0], at(0, 1, 0, 0)).wait_send()
+
+    def b_landed(g, half):
+        place = result.at[RESULT[g], pl.ds(1, 7), pl.ds(0, 2)]
+        remote(place, place, b_send.at[g], b_recv.at[g, half], at(0, 1, 0, 0)).wait_recv()
 
     def second_product(g):
         for way in (2, 3):
             h_copy(g, way, (x + 2) % 4).wait_recv()
         if g >= 2:
-            for dy, dc in Y_ORDER:
-                b_copy(0 if g == 3 else 1, dy, dc).wait_send()
+            b_left(0 if g == 3 else 1)
 
         @pl.loop(0, OUT_PART // 256)
         def _(t):
@@ -327,44 +328,53 @@
                 total += jnp.dot(hidden[g, s], w_down[s * 256 : (s + 1) * 256, cols], preferred_element_type=F32)
             result[RESULT[g], :, :, :, cols] = total.astype(BF16).reshape(8, 4, CAP, 256)
 
-        for dy, dc in Y_ORDER:
-            b_copy(g, dy, dc).start()
+        for half in range(2):
+            for dy, dc in Y_ORDER:
+                b_copy(g, dy, dc, half).start()
         back[g, :, y * 2 + c] = result[RESULT[g], 0]
 
-    def p_copy(g):
-        return remote(partial.at[g - 1], landed.at[g - 1], p_send.at[g], p_recv.at[g], at(4 - g, 0, 0, 0))
+    def p_copy(g, half):
+        r = pl.ds(half * 256, 256)
+        return remote(
+            partial.at[g - 1, r], landed.at[g - 1, r], p_send.at[g], p_recv.at[g, half], at(4 - g, 0, 0, 0)
+        )
+
+    def p_left(g):
+        sent = partial.at[g - 1]
+        remote(sent, sent, p_send.at[g], p_recv.at[g, 0], at(1, 0, 0, 0)).wait_send()
 
     def combine(g):
-        for dy, dc in Y_ORDER:
-            b_landing(g, dy, dc).wait_recv()
-
-        @pl.loop(0, 4)
-        def _(q):
-            weight = jnp.where(slot_row == meta[g, q, 0:1, :] - plane, meta[g, q, 2:3, :], 0.0)
-            weight = weight + jnp.where(slot_row == meta[g, q, 1:2, :] - plane, meta[g, q, 3:4, :], 0.0)
-            high = weight.astype(BF16)
-            low = (weight - high.astype(F32)).astype(BF16)
-            rows = back[g, q].reshape(128, OUT_PART)
-            dims = (((0,), (0,)), ((), ()))
-            total = lax.dot_general(high, rows, dims, preferred_element_type=F32)
-            total += lax.dot_general(low, rows, dims, preferred_element_type=F32)
-            r = pl.ds(pl.multiple_of(q * 128, 128), 128)
+        for half in range(2):
+            b_landed(g, half)
+
+            @pl.loop(half * 2, half * 2 + 2)
+            def _(q):
+                weight = jnp.where(slot_row == meta[g, q, 0:1, :] - plane, meta[g, q, 2:3, :], 0.0)
+                weight = weight + jnp.where(slot_row == meta[g, q, 1:2, :] - plane, meta[g, q, 3:4, :], 0.0)
+                high = weight.astype(BF16)
+                low = (weight - high.astype(F32)).astype(BF16)
+                rows = back[g, q].reshape(128, OUT_PART)
+                dims = (((0,), (0,)), ((), ()))
+                total = lax.dot_general(high, rows, dims, preferred_element_type=F32)
+                total += lax.dot_general(low, rows, dims, preferred_element_type=F32)
+                r = pl.ds(pl.multiple_of(q * 128, 128), 128)
+                if g:
+                    partial[g - 1, r, :] = total.astype(BF16)
+                else:
+                    out[r, :] = total.astype(BF16)
+
             if g:
-                partial[g - 1, r, :] = total.astype(BF16)
-            else:
-                out[r, :] = total.astype(BF16)
-
-        if g:
-            p_copy(g).start()
+                p_copy(g, half).start()
 
     def out_store(part):
         r = pl.ds(part * 128, 128)
-        return pltpu.make_async_copy(out.at[r], out_hbm.at[r], out_sem.at[part])
+        return pltpu.make_async_copy(out.at[r], out_hbm.at[r], out_sem)
 
     def final_sum():
-        for g in (1, 3, 2):
-            p_copy(g).wait_recv()
         for part in range(4):
+            if part % 2 == 0:
+                for g in (1, 3, 2):
+                    p_copy(g, part // 2).wait_recv()
 
             @pl.loop(0, 4)
             def _(t):
@@ -450,18 +460,22 @@
         return remote(
             gated.at[pl.ds(b * BLOCK, BLOCK)],
             held(x, b),
-            c_send.at[way, b],
+            c_send.at[way],
             c_recv.at[way, b],
             at(0, 0, 0, 1 if way == 0 else 3),
         )
 
     def c_landing(way, b):
         place = held((x + 3) % 4 if way == 0 else (x + 1) % 4, b)
-        return remote(place, place, c_send.at[way, b], c_recv.at[way, b], at(0, 0, 0, 1 if way == 0 else 3))
+        return remote(place, place, c_send.at[way], c_recv.at[way, b], at(0, 0, 0, 1 if way == 0 else 3))
 
     def c_pass(way, part, source):
         place = held(source, way - 2) if part == 0 else held(source, 2, (way - 2) * 64, 64)
-        return remote(place, place, c_send.at[way, part], c_recv.at[way, part], at(0, 0, 0, 1 if way == 2 else 3))
+        return remote(place, place, c_send.at[way], c_recv.at[way, part], at(0, 0, 0, 1 if way == 2 else 3))
+
+    def c_left(way, rows):
+        sent = gated.at[pl.ds(0, rows)]
+        remote(sent, sent, c_send.at[way], c_recv.at[way, 0], at(0, 0, 0, 1)).wait_send()
 
     def free_tokens():
         for dz in (1, 2, 3):
@@ -496,8 +510,12 @@
         return pltpu.make_async_copy(
             slots.at[buffer, :, cols],
             conv_out.at[pl.ds(pl.multiple_of(source * ROWS + b * BLOCK, BLOCK), BLOCK)],
-            store_sem.at[dx, b],
-        )
+            store_sem.at[dx],
+        )
+
+    def conv_stored(dx):
+        rows = conv_out.at[pl.ds(0, ROWS)]
+        pltpu.make_async_copy(rows, rows, store_sem.at[dx]).wait()
 
     def conv_product(dx, blocks=(0, 1, 2)):
         source = (x + dx) % 4
@@ -524,42 +542,34 @@
 
             conv_store(dx, b).start()
 
-    def y_left():
+    def all_y_left():
         for dz in range(1, 4):
             for i in range(2):
-                for dy, dc in Y_ORDER:
-                    y_copy(dz, i, dy, dc).wait_send()
+                y_left(dz, i)
 
     def drain():
         for dz in (1, 2, 3):
             meta_copies[dz].wait_send()
         halo.wait_send()
         for g in range(4):
-            for way in range(4):
-                h_copy(g, way, (x, x, (x + 3) % 4, (x + 1) % 4)[way]).wait_send()
+            sent = hidden.at[g, pl.ds(0, 3)]
+            remote(sent, sent, h_send.at[g], h_recv.at[g, 0], at(0, 0, 0, 1)).wait_send()
             if g >= 2:
-                for dy, dc in Y_ORDER:
-                    b_copy(g, dy, dc).wait_send()
+                b_left(g)
             for i in range(2):
-                for k in range(8):
-                    x_copy(g, i, k).wait_send()
+                x_left(g, i)
         for way in range(2):
-            for b in range(3):
-                c_copy(way, b).wait_send()
+            c_left(way, ROWS)
         for dx in (0, 1, 3):
-            for b in range(3):
-                conv_store(dx, b).wait()
+            conv_stored(dx)
 
     def finish():
         for dz in (1, 2, 3):
-            p_copy(dz).wait_send()
-        for way in range(2):
-            for part in range(2):
-                c_pass(way + 2, part, (x + 3) % 4 if way == 0 else (x + 1) % 4).wait_send()
-        for part in range(4):
-            out_store(part).wait()
-        for b in range(3):
-            conv_store(2, b).wait()
+            p_left(dz)
+        for way in (2, 3):
+            c_left(way, ROWS // 2)
+        pltpu.make_async_copy(out, out_hbm, out_sem).wait()
+        conv_stored(2)
 
     def build_pair(number):
         for dz, i in PAIRS[number]:
@@ -601,9 +611,8 @@
             0: [lambda: pass_hidden(0)],
             1: [lambda: first_product(1)],
             2: [lambda: first_product(3)],
-            3: [lambda: second_product(0)],
-            5: [lambda: pass_hidden(1)],
-            6: [lambda: pass_hidden(3)],
+            4: [lambda: pass_hidden(1), lambda: second_product(0)],
+            5: [lambda: pass_hidden(3)],
         },
     )
     free_tokens()
@@ -614,17 +623,17 @@
     combine(1)
     pass_hidden(2)
     conv_send()
+    second_product(2)
     combine(3)
-    second_product(2)
-    y_left()
+    combine(2)
+    all_y_left()
+    conv_pass()
     conv_product(0)
-    combine(2)
-    conv_pass()
     conv_product(3)
     conv_product(1)
     drain()
+    conv_product(2, (0, 1))
     final_sum()
-    conv_product(2, (0, 1))
     conv_product(2, (2,))
     finish()
 
@@ -639,7 +648,7 @@
             jax.ShapeDtypeStruct((4 * ROWS, OUT_PART), BF16),
             jax.ShapeDtypeStruct((512, OUT_PART), BF16),
         ),
-        in_specs=[hbm, hbm, vmem, vmem, vmem, hbm, hbm, vmem, vmem, vmem, hbm, hbm, hbm],
+        in_specs=[hbm, hbm, vmem, vmem, vmem, hbm, hbm, vmem, vmem, vmem, vmem, hbm, hbm, hbm],
         out_specs=(hbm, hbm),
         scratch_shapes=[
             pltpu.VMEM((4, 2, 128, D), BF16),
@@ -665,21 +674,21 @@
             dma((4, 2)),
             dma((4,)),
             dma((4,)),
+            dma((4, 2)),
             dma((4, 2, 8)),
-            dma((4, 2, 8)),
-            dma((4, 2, 8)),
-            dma((4, 2, 8)),
+            dma((4, 2)),
+            dma((4, 2)),
+            dma((4,)),
             dma((4, 4)),
-            dma((4, 4)),
-            dma((4, 8)),
-            dma((4, 8)),
             dma((4,)),
+            dma((4, 2)),
             dma((4,)),
+            dma((4, 2)),
             dma((2,)),
-            dma((4, 3)),
-            dma((4, 3)),
+            dma((4,)),
             dma((4, 3)),
             dma((4,)),
+            dma(()),
             pltpu.SemaphoreType.REGULAR,
         ],
         compiler_params=pltpu.CompilerParams(
@@ -705,9 +714,6 @@
     up_weight,
     down_weight,
 ):
-    route_share = group_gate[:, None] * expert_gate / jnp.sum(expert_gate, axis=1, keepdims=True)
-    route = route_experts.reshape(4, MOE_DEV, TOP).transpose(0, 2, 1)
-    share = route_share.reshape(4, MOE_DEV, TOP).transpose(0, 2, 1)
     return both_branches(
         conv_value,
         conv_gate,
@@ -717,8 +723,9 @@
         conv_projection,
         expert_input,
         expert_gain[None],
-        route,
-        share,
+        route_experts.T,
+        group_gate[None],
+        expert_gate.T,
         gate_weight,
         up_weight,
         down_weight,

time: 225 us -> 216 us (0.960)
  Pallas kernels: 216 us -> 211 us
    pallas_call x1, Pallas kernels: 216 us -> 211 us  [both_branches(): pl.pallas_call(kernel, name='experts', out_shape=(jax.ShapeDtypeStruct((4...]
where the time goes in v3:
time: 216 us
  Pallas kernels  211 us (98%)
  local copies, waits for them, and re-layouts  4.92 us (2%)
    pallas_call x1, Pallas kernels, both_branches(): pl.pallas_call(kernel, name='experts', out_shape=(jax.ShapeDtypeStruct((4...  211 us
    unnamed x4, local copies, waits for them, and re-layouts  4.92 us

profile of v3, /device:TPU:1, one launch (start us, length us, event | category | flops | bytes accessed | tf_op | source)
XLA Modules:
  0.0 216.1 jit_solution(1995001865065007354)
XLA Ops:
  0.6 210.5 %experts.1 = (bf16[1536,1024]{1,0:T(8,128)(2,1)}, bf16[512,1024]{1,0:T(8,128)(2,1)}) custom-call(bf16[384,2048]{1,0:T(8,128)(2,1)} %value_hbm.1, bf16[384,2048]{1,0:T(8,128)(2,1)} %gate_rows_hbm.1, f32[31,2048]{1,0:T(8,128)} %taps.1, f32[1,2048]{1,0:T(1,128)} %bitcast.7, f32[1,2048]{1,0:T(1,128)} %bitcast.8, bf16[2048,1024]{1,0:T(8,128)(2,1)} %projection_hbm.1, ...), custom_call_target="tpu_custom_call" | custom-call | flops 149999992832 | bytes 16777216 | tf_op jit(solution)/shard_map/experts/pallas_call | solution.py:644
  211.2 0.0 copy-start
  211.2 3.9 %copy.18 = bf16[1536,1024]{1,0:T(8,128)(2,1)} copy(bf16[1536,1024]{1,0:T(8,128)(2,1)} %get-tuple-element.4) | data formatting | bytes 6291456
  215.1 0.0 copy-done
  215.1 1.0 copy.19
Async XLA Ops:
  211.2 4.0 %copy-start = (bf16[512,1024]{1,0:T(8,128)(2,1)S(1)}, bf16[512,1024]{1,0:T(8,128)(2,1)}, u32[]{:S(2)}) copy-start(bf16[512,1024]{1,0:T(8,128)(2,1)} %get-tuple-element.5) | copy-start | bytes 3145732

commit v4 on v3

--- a/solution.py
+++ b/solution.py
@@ -260,6 +260,9 @@
         x_all(dz, i, quarter[i]).wait_send()
 
     def h_copy(g, way, source):
+        if g == 2 and way == 2:
+            piece = hidden.at[g, source]
+            return remote(piece, piece, h_send.at[g], h_recv.at[g, way], at(0, 0, 0, 2))
         half = pl.ds(0, 512) if way < 2 else pl.ds((way - 2) * 256, 256)
         piece = hidden.at[g, source, half]
         return remote(
@@ -287,14 +290,16 @@
             gate = acc_gate[r, :]
             hidden[g, x, r, :] = (gate / (1.0 + jnp.exp(-gate)) * acc_up[r, :]).astype(BF16)
 
-        for way in (0, 1):
+        for way in (0, 1, 2) if g == 2 else (0, 1):
             h_copy(g, way, x).start()
 
     def pass_hidden(g):
         h_copy(g, 0, (x + 3) % 4).wait_recv()
-        h_copy(g, 2, (x + 3) % 4).start()
+        if g != 2:
+            h_copy(g, 2, (x + 3) % 4).start()
         h_copy(g, 1, (x + 1) % 4).wait_recv()
-        h_copy(g, 3, (x + 1) % 4).start()
+        if g != 2:
+            h_copy(g, 3, (x + 1) % 4).start()
 
     def b_copy(g, dy, dc, half):
         pick = pl.ds(half * 2, 2)
@@ -315,7 +320,7 @@
         remote(place, place, b_send.at[g], b_recv.at[g, half], at(0, 1, 0, 0)).wait_recv()
 
     def second_product(g):
-        for way in (2, 3):
+        for way in (2,) if g == 2 else (2, 3):
             h_copy(g, way, (x + 2) % 4).wait_recv()
         if g >= 2:
             b_left(0 if g == 3 else 1)
@@ -620,9 +625,9 @@
     second_product(3)
     combine(0)
     first_product(2)
+    conv_send()
     combine(1)
     pass_hidden(2)
-    conv_send()
     second_product(2)
     combine(3)
     combine(2)

time: 216 us -> 219 us (1.014)
  no operation moved by 1% of the time
where the time goes in v4:
time: 219 us; the launch traced here: 218 us
  Pallas kernels  212 us (97%)
  local copies, waits for them, and re-layouts  4.92 us (2%)
    pallas_call x1, Pallas kernels, both_branches(): pl.pallas_call(kernel, name='experts', out_shape=(jax.ShapeDtypeStruct((4...  212 us
    unnamed x4, local copies, waits for them, and re-layouts  4.92 us

profile of v4, /device:TPU:1, one launch (start us, length us, event | category | flops | bytes accessed | tf_op | source)
XLA Modules:
  0.0 217.8 jit_solution(9242747324120181374)
XLA Ops:
  0.6 212.2 %experts.1 = (bf16[1536,1024]{1,0:T(8,128)(2,1)}, bf16[512,1024]{1,0:T(8,128)(2,1)}) custom-call(bf16[384,2048]{1,0:T(8,128)(2,1)} %value_hbm.1, bf16[384,2048]{1,0:T(8,128)(2,1)} %gate_rows_hbm.1, f32[31,2048]{1,0:T(8,128)} %taps.1, f32[1,2048]{1,0:T(1,128)} %bitcast.7, f32[1,2048]{1,0:T(1,128)} %bitcast.8, bf16[2048,1024]{1,0:T(8,128)(2,1)} %projection_hbm.1, ...), custom_call_target="tpu_custom_call" | custom-call | flops 149999992832 | bytes 16777216 | tf_op jit(solution)/shard_map/experts/pallas_call | solution.py:649
  212.9 0.0 copy-start
  212.9 3.9 %copy.18 = bf16[1536,1024]{1,0:T(8,128)(2,1)} copy(bf16[1536,1024]{1,0:T(8,128)(2,1)} %get-tuple-element.4) | data formatting | bytes 6291456
  216.8 0.0 copy-done
  216.8 1.0 copy.19
Async XLA Ops:
  212.9 4.0 %copy-start = (bf16[512,1024]{1,0:T(8,128)(2,1)S(1)}, bf16[512,1024]{1,0:T(8,128)(2,1)}, u32[]{:S(2)}) copy-start(bf16[512,1024]{1,0:T(8,128)(2,1)} %get-tuple-element.5) | copy-start | bytes 3145732
